TPU v7x, 32 devices: a whole 2x2x4 slice. The times are simulated.
32 devices in a mesh: ep: 8 (over z, x), tp: 4 (over y, core).
Axes of the slice: x: 2, y: 2, z: 4, core: 2. Of those that a mesh axis runs over, the one named last changes fastest.
Arguments:
- tokens: bfloat16 [2048, 2048], P('ep'), may hold values from -6 to 6
- routes: int32 [2048, 2], P('ep'), may hold values from 0 to 7, all different within a row; in each aligned block of 256 rows (0 to 255, 256 to 511, ...) at most 128 rows name the same one
- router_matrix: bfloat16 [2048, 8], replicated, may hold values from -0.125 to 0.125
- cotangent: bfloat16 [2048, 2048], P('ep', 'tp'), may hold values from -3 to 3
- gate_proj: bfloat16 [8, 2048, 3584], P('ep', None, 'tp'), may hold values from -0.125 to 0.125
- up_proj: bfloat16 [8, 2048, 3584], P('ep', None, 'tp'), may hold values from -0.125 to 0.125
- down_proj: bfloat16 [8, 3584, 2048], P('ep', 'tp'), may hold values from -0.09375 to 0.09375
Outputs:
- token_grad: bfloat16 [2048, 2048], P('ep', 'tp')
- mixing_grad: float32 [2048, 2], P('ep')
- router_grad: float32 [2048, 8], P(('ep', 'tp'))
- gate_grad: bfloat16 [8, 2048, 3584], P('ep', None, 'tp')
- up_grad: bfloat16 [8, 2048, 3584], P('ep', None, 'tp')
- down_grad: bfloat16 [8, 3584, 2048], P('ep', 'tp')
Inputs may be any that keep to these rules, and one draw needn't show every extreme that they name: `routes`: the two experts of a row differ. In each aligned block of 256 rows no expert is named by more than 128 rows, a bound that some block reaches; every expert is named somewhere.
All inputs are finite; a program needn't handle non-finite values.
Results may differ from a plain program's by a relative error of at most 0.019.
Values may be sent and summed in bfloat16 or wider, within the bound.
A program may use at most 128 MiB of HBM per device.

v0:
```python
import math

import jax
import jax.numpy as jnp
from jax import lax
from jax.experimental import pallas as pl
from jax.experimental.pallas import tpu as pltpu
from jax.sharding import PartitionSpec as P

MESH = pl.DeviceIdType.MESH
LANES = 128


def remote(src, dst, send, recv, ep, tp):
    return pltpu.make_async_remote_copy(
        src_ref=src,
        dst_ref=dst,
        send_sem=send,
        recv_sem=recv,
        device_id=(ep, tp),
        device_id_type=MESH,
    )


def pair(me, k, size):
    if size & (size - 1):
        return lax.rem(me + k, size)
    return sum((me // bit + k // bit) % 2 * bit for bit in (1 << b for b in range(size.bit_length() - 1)))


def came(me, k, size):
    if size & (size - 1):
        return lax.rem(me + size - k, size)
    return pair(me, k, size)


def greet(me, tp, senders, peers):
    barrier = pltpu.get_barrier_semaphore()

    def hello(k, carry):
        pl.semaphore_signal(barrier, inc=1, device_id=(pair(me, k, senders), tp), device_id_type=MESH)
        return carry

    lax.fori_loop(1, senders, hello, 0)
    for peer in peers:
        pl.semaphore_signal(barrier, inc=1, device_id=(me, peer), device_id_type=MESH)
    pl.semaphore_wait(barrier, senders - 1 + len(peers))


def span(start, size):
    return pl.ds(pl.multiple_of(start * size, size), size)


def dispatch_kernel(senders, rows, capacity, col):
    def body(tok_ref, cot_ref, mix_ref, tok_out, cot_out, mix_out, ep_send, ep_recv, y_send, y_recv,
             c_send, c_recv, m_send, m_recv, l_sem):
        me = lax.axis_index("ep")
        tp = lax.axis_index("tp")
        row = tp // 2
        core = tp % 2
        partner = row * 2 + (1 - core)

        def seat(step, side):
            return lax.rem(row + step + rows, rows) * 2 + side

        greet(me, tp, senders, [partner] + [seat(j, core) for j in range(1, rows)])

        def piece(out, block, tp_col):
            return out.at[span(block, capacity), span(tp_col, col)]

        def source(array, dest, tp_col):
            if array == 0:
                return tok_ref.at[dest, :, span(tp_col // 2, col)]
            return cot_ref.at[dest]

        far = [(1, 0), (0, 0)]
        near = far + [(0, j) for j in range(1, rows)]
        far_hops = [(a, j) for j in range(1, rows) for a in (1, 0)]
        near_hops = [(1, j) for j in range(1, rows)]
        half = max(senders // 2, 1)
        outs = (tok_out, cot_out)

        def ep_copy(i, dest, block):
            array, which = near[i]
            return remote(source(array, dest, seat(which, core)), piece(outs[array], block, seat(which, core)),
                          ep_send.at[i, dest], ep_recv.at[i, block], dest, tp)

        def mix_copy(dest, block):
            return remote(mix_ref.at[dest], mix_out.at[block], m_send.at[dest], m_recv.at[block], dest, tp)

        def local_copy(i):
            array, which = near[i]
            return pltpu.make_async_copy(source(array, me, seat(which, core)),
                                         piece(outs[array], me, seat(which, core)), l_sem.at[i])

        local_mix = pltpu.make_async_copy(mix_ref.at[me], mix_out.at[me], l_sem.at[len(near)])

        def y_copy(array, step, block):
            place = piece(outs[array], block, tp)
            return remote(place, place, y_send.at[array, step, block], y_recv.at[array, step, block],
                          me, seat(step, core))

        def y_arrival(array, step, block):
            place = piece(outs[array], block, seat(-step, core))
            return remote(place, place, y_send.at[array, step, block], y_recv.at[array, step, block],
                          me, seat(step, core))

        def c_copy(array, step, block):
            place = piece(outs[array], block, seat(step, core))
            return remote(place, place, c_send.at[array, step + rows, block],
                          c_recv.at[array, step + rows, block], me, partner)

        def c_arrival(array, step, block):
            place = piece(outs[array], block, seat(step, 1 - core))
            return remote(place, place, c_send.at[array, step + rows, block],
                          c_recv.at[array, step + rows, block], me, partner)

        relays = far + [(array, -step) for array, step in far_hops]
        near_relays = near + [(array, -step) for array, step in near_hops]

        def send_all(count):
            def step(k, carry):
                dest = pair(me, k, senders)
                for i in range(count):
                    ep_copy(i, dest, me).start()
                mix_copy(dest, me).start()
                return carry

            return step

        lax.fori_loop(1, half, send_all(len(near)), 0)
        lax.fori_loop(half, senders, send_all(len(far)), 0)
        for i in range(len(near)):
            local_copy(i).start()
        local_mix.start()
        for i in range(len(near)):
            local_copy(i).wait()
        local_mix.wait()

        def spread(block, items, hops):
            for array, step in hops:
                y_copy(array, step, block).start()
            for array, step in items:
                c_copy(array, step, block).start()

        def pass_on(block, hops):
            for array, step in hops:
                y_arrival(array, step, block).wait_recv()
                c_copy(array, -step, block).start()

        spread(me, near, near_hops)

        def relay(items, hops, past_hops):
            def step(k, carry):
                block = came(me, k, senders)
                for i in range(len(items)):
                    ep_copy(i, block, block).wait_recv()
                spread(block, items, hops)
                pass_on(came(me, k - 1, senders), past_hops)
                return carry

            return step

        lax.fori_loop(1, half, relay(near, near_hops, near_hops), 0)
        lax.fori_loop(half, min(half + 1, senders), relay(far, far_hops, near_hops), 0)
        lax.fori_loop(half + 1, senders, relay(far, far_hops, far_hops), 0)
        pass_on(came(me, senders - 1, senders), far_hops if senders > 1 else near_hops)

        def finish(through, hops):
            def step(k, carry):
                block = came(me, k, senders)
                for array, step in through:
                    c_arrival(array, step, block).wait_recv()
                    c_copy(array, step, block).wait_send()
                for array, step in hops:
                    y_copy(array, step, block).wait_send()
                return carry

            return step

        lax.fori_loop(0, half, finish(near_relays, near_hops), 0)
        lax.fori_loop(half, senders, finish(relays, far_hops), 0)

        def finish_ep(count):
            def step(k, carry):
                dest, block = pair(me, k, senders), came(me, k, senders)
                for i in range(count):
                    ep_copy(i, dest, me).wait_send()
                mix_copy(dest, me).wait_send()
                mix_copy(block, block).wait_recv()
                return carry

            return step

        lax.fori_loop(1, half, finish_ep(len(near)), 0)
        lax.fori_loop(half, senders, finish_ep(len(far)), 0)

    return body


def dispatch(tok_send, cot_send, mix_send):
    senders, capacity, col = cot_send.shape
    width = col * lax.axis_size("tp")
    n_rows = lax.axis_size("tp") // 2
    vmem = pl.BlockSpec(memory_space=pltpu.VMEM)
    dma = pltpu.SemaphoreType.DMA
    rows = jax.ShapeDtypeStruct((senders * capacity, width), cot_send.dtype)
    return pl.pallas_call(
        dispatch_kernel(senders, n_rows, capacity, col),
        out_shape=(rows, rows, jax.ShapeDtypeStruct(mix_send.shape, mix_send.dtype)),
        in_specs=[vmem] * 3,
        out_specs=[pl.BlockSpec(memory_space=pl.ANY)] * 2 + [vmem],
        scratch_shapes=[
            dma((2 + n_rows, senders)), dma((2 + n_rows, senders)),
            dma((2, n_rows, senders)), dma((2, n_rows, senders)),
            dma((2, 2 * n_rows, senders)), dma((2, 2 * n_rows, senders)),
            dma((senders,)), dma((senders,)),
            dma((3 + n_rows,)),
        ],
        compiler_params=pltpu.CompilerParams(has_side_effects=True, collective_id=0, vmem_limit_bytes=24 << 20),
        name="dispatch",
    )(tok_send, cot_send, mix_send)


def combine_kernel(senders, rows, capacity, col):
    def body(terms, mix_ref, out, mix_out, c_buf, y_src, y_buf, fin, mix_got, mix_all,
             c_send, c_recv, y_send, y_recv, h_send, h_recv, m_send, m_recv, t_send, t_recv):
        me = lax.axis_index("ep")
        tp = lax.axis_index("tp")
        row = tp // 2
        core = tp % 2
        partner = row * 2 + (1 - core)

        def seat(step, side):
            return lax.rem(row + step + rows, rows) * 2 + side

        greet(me, tp, senders, [lax.rem(tp + k, 2 * rows) for k in range(1, 2 * rows)])

        def c_copy(step, block):
            return remote(terms.at[block, :, span(seat(step, 1 - core), col)], c_buf.at[step, block],
                          c_send.at[step, block], c_recv.at[step, block], me, partner)

        def y_copy(step, block):
            return remote(y_src.at[step - 1, block], y_buf.at[step - 1, block],
                          y_send.at[step, block], y_recv.at[step, block], me, seat(step, core))

        def h_copy(dest, slot):
            return remote(fin.at[dest], out.at[slot], h_send.at[dest], h_recv.at[slot], dest, tp)

        def m_copy(dest, slot):
            return remote(mix_ref.at[dest], mix_got.at[slot], m_send.at[dest], m_recv.at[slot], dest, tp)

        def order(k):
            return pair(me, senders - k, senders)

        def start(k, carry):
            for step in list(range(1, rows)) + [0]:
                c_copy(step, order(k)).start()
            return carry

        lax.fori_loop(1, senders + 1, start, 0)

        def start_mix(k, carry):
            m_copy(order(k), me).start()
            return carry

        lax.fori_loop(1, senders, start_mix, 0)
        mix_got[me] = mix_ref[me]

        def first(block):
            for step in range(1, rows):
                c_copy(step, block).wait_recv()
                y_src[step - 1, block] = (
                    terms[block, :, span(seat(step, core), col)].astype(jnp.float32)
                    + c_buf[step, block].astype(jnp.float32)
                ).astype(y_src.dtype)
                y_copy(step, block).start()

        def total(block):
            c_copy(0, block).wait_recv()
            value = terms[block, :, span(tp, col)].astype(jnp.float32) + c_buf[0, block].astype(
                jnp.float32
            )
            for step in range(1, rows):
                y_copy(step, block).wait_recv()
                value = value + y_buf[step - 1, block].astype(jnp.float32)
            return value.astype(out.dtype)

        def second(block):
            fin[block] = total(block)
            h_copy(block, me).start()

        ahead = 2

        def lead(k, carry):
            first(order(k))
            return carry

        def steady(k, carry):
            first(order(k))
            second(order(k - ahead))
            return carry

        lax.fori_loop(1, 1 + ahead, lead, 0)
        lax.fori_loop(1 + ahead, senders + 1, steady, 0)

        def last(k, carry):
            second(order(k))
            return carry

        lax.fori_loop(senders + 1 - ahead, senders, last, 0)
        out[me] = total(me)

        def mix_arrive(k, carry):
            m_copy(order(k), order(k)).wait_recv()
            return carry

        lax.fori_loop(1, senders, mix_arrive, 0)
        mix_all[0] = mix_got[...]

        def t_copy(k):
            peer = lax.rem(tp + k, 2 * rows)
            return remote(mix_got, mix_all.at[k], t_send.at[k], t_recv.at[k], me, peer)

        for k in range(1, 2 * rows):
            t_copy(k).start()

        def finish(k, carry):
            block = order(k)
            for step in range(rows):
                c_copy(step, block).wait_send()
            for step in range(1, rows):
                y_copy(step, block).wait_send()
            return carry

        lax.fori_loop(0, senders, finish, 0)

        def finish_home(k, carry):
            block = order(k)
            h_copy(block, block).wait()
            m_copy(block, block).wait_send()
            return carry

        lax.fori_loop(1, senders, finish_home, 0)
        for k in range(1, 2 * rows):
            t_copy(k).wait()
        mix_out[...] = jnp.sum(mix_all[...], axis=0)

    return body


def combine(terms, mix_part):
    senders, capacity, width = terms.shape
    col = width // lax.axis_size("tp")
    n_rows = lax.axis_size("tp") // 2
    vmem = pl.BlockSpec(memory_space=pltpu.VMEM)
    dma = pltpu.SemaphoreType.DMA
    block = (senders, capacity, col)
    return pl.pallas_call(
        combine_kernel(senders, n_rows, capacity, col),
        out_shape=(
            jax.ShapeDtypeStruct(block, terms.dtype),
            jax.ShapeDtypeStruct(mix_part.shape, mix_part.dtype),
        ),
        in_specs=[vmem] * 2,
        out_specs=[vmem] * 2,
        scratch_shapes=[
            pltpu.VMEM((n_rows,) + block, terms.dtype),
            pltpu.VMEM((n_rows - 1,) + block, terms.dtype),
            pltpu.VMEM((n_rows - 1,) + block, terms.dtype),
            pltpu.VMEM(block, terms.dtype),
            pltpu.VMEM(mix_part.shape, mix_part.dtype),
            pltpu.VMEM((2 * n_rows,) + mix_part.shape, mix_part.dtype),
            dma((n_rows, senders)), dma((n_rows, senders)),
            dma((n_rows, senders)), dma((n_rows, senders)),
            dma((senders,)), dma((senders,)),
            dma((senders,)), dma((senders,)),
            dma((2 * n_rows,)), dma((2 * n_rows,)),
        ],
        compiler_params=pltpu.CompilerParams(has_side_effects=True, collective_id=1, vmem_limit_bytes=32 << 20),
        name="combine",
    )(terms, mix_part)


def router_sum(terms):
    senders = terms.shape[0]

    def body(src, out, got, send, recv):
        me = lax.axis_index("ep")
        tp = lax.axis_index("tp")

        greet(me, tp, senders, [])

        def copy(dest, slot):
            return remote(src.at[dest], got.at[slot], send.at[dest], recv.at[slot], dest, tp)

        def start(k, carry):
            copy(lax.rem(me + k, senders), me).start()
            return carry

        lax.fori_loop(1, senders, start, 0)
        got[me] = src[me]

        def wait(k, carry):
            block = lax.rem(me + k, senders)
            copy(block, block).wait()
            return carry

        lax.fori_loop(1, senders, wait, 0)
        out[...] = jnp.sum(got[...], axis=0)

    vmem = pl.BlockSpec(memory_space=pltpu.VMEM)
    dma = pltpu.SemaphoreType.DMA
    return pl.pallas_call(
        body,
        out_shape=jax.ShapeDtypeStruct(terms.shape[1:], terms.dtype),
        in_specs=[vmem],
        out_specs=vmem,
        scratch_shapes=[pltpu.VMEM(terms.shape, terms.dtype), dma((senders,)), dma((senders,))],
        compiler_params=pltpu.CompilerParams(has_side_effects=True, collective_id=2, vmem_limit_bytes=8 << 20),
        name="router_sum",
    )(terms)


def slot_places(flat_routes, experts, capacity):
    entries = flat_routes.shape[0]
    onehot = flat_routes[:, None] == jnp.arange(experts, dtype=jnp.int32)[None, :]
    index = jnp.arange(entries, dtype=jnp.int32)
    before = (index[None, :] < index[:, None]).astype(jnp.bfloat16)
    earlier = jnp.dot(before, onehot.astype(jnp.bfloat16), preferred_element_type=jnp.float32)
    rank = jnp.sum(jnp.where(onehot, earlier, 0.0), axis=1).astype(jnp.int32)
    return flat_routes * capacity + rank


def pad_lanes(rows):
    return jnp.pad(rows[:, None, :], ((0, 0), (0, 7), (0, LANES - rows.shape[1])))


def local(tokens, routes, router_matrix, cotangent, gate_proj, up_proj, down_proj):
    ep_size = lax.axis_size("ep")
    tp_size = lax.axis_size("tp")
    tp_index = lax.axis_index("tp")
    home_rows, model_width = tokens.shape
    top_count = routes.shape[1]
    experts = router_matrix.shape[1]
    capacity = home_rows * top_count * 2 // experts
    col_width = model_width // tp_size
    places = slot_places(routes.reshape(-1), experts, capacity).reshape(home_rows, top_count)
    slot_ids = jnp.arange(experts * capacity, dtype=jnp.int32)
    hits = slot_ids[:, None, None] == places.T[None, :, :]
    pick = jnp.any(hits, axis=1).astype(jnp.bfloat16)
    logits = jnp.dot(tokens, router_matrix, preferred_element_type=jnp.float32)
    picked = routes[:, :, None] == jnp.arange(experts, dtype=jnp.int32)[None, None, :]
    chosen = jnp.sum(jnp.where(picked, logits[:, None, :], 0.0), axis=2)
    mixing = jax.nn.sigmoid(chosen - chosen[:, ::-1])
    mix_send = jnp.sum(jnp.where(hits, mixing.T[None, :, :], 0.0), axis=(1, 2))
    mix_send = pad_lanes(mix_send.reshape(experts, capacity))
    token_cols = lax.dynamic_slice_in_dim(
        tokens.reshape(home_rows, tp_size // 2, 2, col_width), tp_index % 2, 1, 2
    ).reshape(home_rows, model_width // 2)
    token_send = jnp.dot(pick, token_cols, preferred_element_type=jnp.float32).astype(
        jnp.bfloat16
    ).reshape(experts, capacity, -1)
    output_send = jnp.dot(pick, cotangent, preferred_element_type=jnp.float32).astype(
        jnp.bfloat16
    ).reshape(experts, capacity, col_width)
    token_rows, output_rows, mix_in = dispatch(token_send, output_send, mix_send)
    senders = ep_size
    slots = senders * capacity
    mix_value = mix_in[:, 0, :capacity].reshape(slots).astype(jnp.bfloat16).astype(jnp.float32)
    w_gate = gate_proj[0]
    w_up = up_proj[0]
    w_down = down_proj[0]
    over_rows = (((0,), (0,)), ((), ()))
    over_cols = (((1,), (1,)), ((), ()))
    gate_pre = jnp.dot(token_rows, w_gate, preferred_element_type=jnp.float32)
    up_pre = jnp.dot(token_rows, w_up, preferred_element_type=jnp.float32)
    gate_sig = jax.nn.sigmoid(gate_pre)
    active = gate_pre * gate_sig
    hidden = (active * up_pre).astype(jnp.bfloat16)
    back_hidden = lax.dot_general(
        output_rows, w_down, over_cols, preferred_element_type=jnp.float32
    )
    mix_part = jnp.sum(hidden.astype(jnp.float32) * back_hidden, axis=1)
    scaled = mix_value[:, None] * back_hidden
    gate_back = (scaled * up_pre * gate_sig * (1.0 + gate_pre * (1.0 - gate_sig))).astype(
        jnp.bfloat16
    )
    up_back = (scaled * active).astype(jnp.bfloat16)
    out_scaled = (mix_value[:, None] * output_rows).astype(jnp.bfloat16)
    slot_terms = lax.dot_general(gate_back, w_gate, over_cols, preferred_element_type=jnp.float32)
    slot_terms = slot_terms + lax.dot_general(
        up_back, w_up, over_cols, preferred_element_type=jnp.float32
    )
    gate_grad = lax.dot_general(
        token_rows, gate_back, over_rows, preferred_element_type=jnp.float32
    ).astype(jnp.bfloat16)[None]
    up_grad = lax.dot_general(
        token_rows, up_back, over_rows, preferred_element_type=jnp.float32
    ).astype(jnp.bfloat16)[None]
    down_grad = lax.dot_general(
        hidden, out_scaled, over_rows, preferred_element_type=jnp.float32
    ).astype(jnp.bfloat16)[None]
    back_rows, back_mix = combine(
        slot_terms.astype(jnp.bfloat16).reshape(senders, capacity, model_width),
        pad_lanes(mix_part.reshape(senders, capacity)),
    )
    back_flat = back_rows.reshape(experts * capacity, col_width)
    over_slots = (((0,), (0,)), ((), ()))
    token_part = lax.dot_general(pick, back_flat, over_slots, preferred_element_type=jnp.float32)
    mix_flat = back_mix[:, 0, :capacity].reshape(experts * capacity)
    mixing_grad = jnp.sum(jnp.where(hits, mix_flat[:, None, None], 0.0), axis=0).T
    pairwise = mixing[:, 0] * mixing[:, 1]
    logit_grad = pairwise[:, None] * (mixing_grad - mixing_grad[:, ::-1])
    route_grad = jnp.sum(jnp.where(picked, logit_grad[:, :, None], 0.0), axis=1)
    router_cols = lax.dynamic_slice_in_dim(
        router_matrix, tp_index * col_width, col_width, 0
    ).astype(jnp.float32)
    router_path = jnp.dot(route_grad, router_cols.T, precision=lax.Precision.HIGHEST)
    token_grad = (token_part + router_path).astype(jnp.bfloat16)
    row_share = model_width // (ep_size * tp_size)
    feature_share = lax.dynamic_slice_in_dim(
        tokens.reshape(home_rows, ep_size, tp_size, row_share), tp_index, 1, 2
    )
    feature_share = feature_share.reshape(home_rows, ep_size * row_share).astype(jnp.float32)
    norm_scale = 1.0 / math.sqrt(home_rows * ep_size)
    router_terms = (
        jnp.dot(route_grad.T, feature_share, precision=lax.Precision.HIGHEST) * norm_scale
    )
    router_terms = jnp.swapaxes(router_terms.reshape(experts, ep_size, row_share), 0, 1)
    router_terms = jnp.pad(router_terms, ((0, 0), (0, 0), (0, LANES - row_share)))
    router_grad = router_sum(router_terms)[:, :row_share].T
    return (token_grad, mixing_grad, router_grad, gate_grad, up_grad, down_grad)


def solution(mesh):
    return jax.shard_map(
        local,
        mesh=mesh,
        in_specs=(
            P("ep", None),
            P("ep", None),
            P(),
            P("ep", "tp"),
            P("ep", None, "tp"),
            P("ep", None, "tp"),
            P("ep", "tp", None),
        ),
        out_specs=(
            P("ep", "tp"),
            P("ep", None),
            P(("ep", "tp"), None),
            P("ep", None, "tp"),
            P("ep", None, "tp"),
            P("ep", "tp", None),
        ),
        check_vma=False,
    )
```

profile of v0, /device:TPU:0, one launch (start us, length us, event | category | flops | bytes accessed | tf_op | source)
XLA Modules:
  0.0 169.8 jit_solution(4546116727913991309)
XLA Ops:
  0.6 0.0 copy-start
  0.7 1.6 fusion.20
  2.3 0.7 select_reduce_fusion.3
  3.0 0.1 rev.6
  3.1 0.8 copy.42
  4.0 0.1 eq.44
  4.1 0.3 fusion.14
  4.4 0.1 convert_element_type.73
  4.5 0.1 copy.43
  4.6 0.7 add_bitcast_fusion
  5.3 0.3 select_reduce_fusion.1
  5.6 0.4 fusion.12
  6.0 1.5 copy.44
  7.6 0.0 copy-done
  7.6 0.0 copy-start.4
  7.6 0.4 convolution_convert_fusion.1
  8.0 0.7 convolution_convert_fusion
  8.8 66.7 %dispatch.1 = (bf16[1024,2048]{1,0:T(8,128)(2,1)S(1)}, bf16[1024,2048]{1,0:T(8,128)(2,1)S(1)}, f32[8,8,128]{2,1,0:T(8,128)S(1)}) custom-call(bf16[8,128,1024]{2,1,0:T(8,128)(2,1)S(1)} %bitcast.65, bf16[8,128,512]{2,1,0:T(8,128)(2,1)S(1)} %bitcast.66, f32[8,8,128]{2,1,0:T(8,128)S(1)} %pad.11.mix_ref), custom_call_target="tpu_custom_call" | custom-call | tf_op jit(solution)/shard_map/dispatch/pallas_call | solution.py:208
  75.5 0.0 copy-done.4
  75.6 0.0 copy-start.5
  75.6 4.2 %fusion.4 = f32[1024,896]{0,1:T(8,128)S(1)} fusion(bf16[1024,2048]{1,0:T(8,128)(2,1)S(1)} %get-tuple-element.13, bf16[1,2048,896]{2,1,0:T(8,128)(2,1)S(1)} %copy-done.4), kind=kOutput, calls=%fused_computation.6 | convolution fusion | flops 3758096384 | bytes 11534336 | tf_op jit(solution)/shard_map/dot_general | solution.py:476
  79.8 0.0 copy-done.5
  79.8 0.0 copy-start.3
  79.8 6.0 %fusion.7 = f32[1024,896]{0,1:T(8,128)} fusion(bf16[1024,2048]{1,0:T(8,128)(2,1)S(1)} %get-tuple-element.13, bf16[1,2048,896]{2,1,0:T(8,128)(2,1)S(1)} %copy-done.5), kind=kOutput, calls=%fused_computation.9 | convolution fusion | flops 3758096384 | bytes 11534336 | tf_op jit(solution)/shard_map/dot_general | solution.py:477
  85.8 0.0 copy-done.3
  85.8 8.2 %multiply_reduce_fusion = (f32[1024]{0:T(1024)S(1)}, bf16[1024,896]{0,1:T(8,128)(2,1)}, bf16[1024,896]{0,1:T(8,128)(2,1)S(1)}, bf16[1024,896]{0,1:T(8,128)(2,1)S(1)}) fusion(f32[1024,896]{0,1:T(8,128)} %fusion.7, f32[1024,896]{0,1:T(8,128)S(1)} %fusion.4, f32[1024]{0:T(1024)S(1)} %bitcast.81, bf16[1024,2048]{1,0:T(8,128)(2,1)S(1)} %get-tuple-element.12, ...), kind=kOutput, calls=%fused_computation.16 | convolution fusion | flops 3775527936 | bytes 20717568 | tf_op jit(solution)/shard_map/dot_general | solution.py:481
  94.0 0.0 copy-start.6
  94.0 7.8 %convert_bitcast_fusion = bf16[1,896,2048]{2,1,0:T(8,128)(2,1)} fusion(bf16[1024,896]{0,1:T(8,128)(2,1)} %get-tuple-element.17, bf16[1024,2048]{1,0:T(8,128)(2,1)S(1)} %get-tuple-element.12, f32[1024]{0:T(1024)S(1)} %bitcast.82), kind=kOutput, calls=%fused_computation.13 | convolution fusion | flops 3766222848 | bytes 9703424 | tf_op jit(solution)/shard_map/dot_general | solution.py:501
  101.8 6.0 %convert_bitcast_fusion.2 = bf16[1,2048,896]{2,1,0:T(8,128)(2,1)} fusion(bf16[1024,2048]{1,0:T(8,128)(2,1)S(1)} %get-tuple-element.13, bf16[1024,896]{0,1:T(8,128)(2,1)S(1)} %get-tuple-element.18), kind=kOutput, calls=%fused_computation.15 | convolution fusion | flops 3759931392 | bytes 9699328 | tf_op jit(solution)/shard_map/dot_general | solution.py:495
  107.8 0.0 copy-done.6
  107.8 6.0 %convert_bitcast_fusion.1 = bf16[1,2048,896]{2,1,0:T(8,128)(2,1)} fusion(bf16[1024,2048]{1,0:T(8,128)(2,1)S(1)} %get-tuple-element.13, bf16[1024,896]{0,1:T(8,128)(2,1)S(1)} %get-tuple-element.19), kind=kOutput, calls=%fused_computation.14 | convolution fusion | flops 3759931392 | bytes 9699328 | tf_op jit(solution)/shard_map/dot_general | solution.py:498
  113.8 4.6 %fusion.2 = f32[1024,2048]{1,0:T(8,128)S(1)} fusion(bf16[1024,896]{0,1:T(8,128)(2,1)S(1)} %get-tuple-element.18, bf16[1,2048,896]{2,1,0:T(8,128)(2,1)S(1)} %copy-done.4), kind=kOutput, calls=%fused_computation.4 | convolution fusion | flops 3758096384 | bytes 13893632 | tf_op jit(solution)/shard_map/dot_general | solution.py:491
  118.4 6.4 %add_convert_fusion = bf16[1024,2048]{1,0:T(8,128)(2,1)S(1)} fusion(f32[1024,2048]{1,0:T(8,128)S(1)} %fusion.2, bf16[1024,896]{0,1:T(8,128)(2,1)} %copy-done.6, bf16[1,2048,896]{2,1,0:T(8,128)(2,1)S(1)} %copy-done.5), kind=kOutput, calls=%fused_computation.1 | convolution fusion | flops 3762290688 | bytes 18087936 | tf_op jit(solution)/shard_map/dot_general | solution.py:492
  124.8 0.0 copy-start.1
  124.8 34.4 %combine.1 = (bf16[8,128,512]{2,1,0:T(8,128)(2,1)S(1)}, f32[8,8,128]{2,1,0:T(8,128)S(1)}) custom-call(bf16[8,128,2048]{2,1,0:T(8,128)(2,1)S(1)} %bitcast.67, f32[8,8,128]{2,1,0:T(8,128)S(1)} %pad.12.mix_ref), custom_call_target="tpu_custom_call" | custom-call | tf_op jit(solution)/shard_map/combine/pallas_call | solution.py:359
  159.3 0.3 select_reduce_fusion
  159.6 0.0 copy-start.2
  159.6 0.1 rev.7
  159.7 0.0 copy-done.1
  159.7 0.3 convolution_multiply_fusion
  160.0 0.1 reshape.67
  160.2 6.7 %router_sum.1 = f32[8,128]{1,0:T(8,128)S(1)} custom-call(f32[8,8,128]{2,1,0:T(8,128)S(1)} %pad.13.src), custom_call_target="tpu_custom_call" | custom-call | tf_op jit(solution)/shard_map/router_sum/pallas_call | solution.py:414
  166.9 0.6 slice_bitcast_fusion
  167.5 1.1 fusion.15
  168.6 1.2 fusion.13
  169.8 0.0 copy-done.2
  (13 shorter events, 0.1 us)
Async XLA Ops:
  0.6 6.9 %copy-start = (bf16[256,512]{1,0:T(8,128)(2,1)S(1)}, bf16[256,512]{1,0:T(8,128)(2,1)}, u32[]{:S(2)}) copy-start(bf16[256,512]{1,0:T(8,128)(2,1)} %param.10) | copy-start | bytes 786436
  7.6 68.0 %copy-start.4 = (bf16[1,2048,896]{2,1,0:T(8,128)(2,1)S(1)}, bf16[1,2048,896]{2,1,0:T(8,128)(2,1)}, u32[]{:S(2)}) copy-start(bf16[1,2048,896]{2,1,0:T(8,128)(2,1)} %param.11) | copy-start | bytes 11010052
  75.6 4.2 %copy-start.5 = (bf16[1,2048,896]{2,1,0:T(8,128)(2,1)S(1)}, bf16[1,2048,896]{2,1,0:T(8,128)(2,1)}, u32[]{:S(2)}) copy-start(bf16[1,2048,896]{2,1,0:T(8,128)(2,1)} %param.12) | copy-start | bytes 11010052
  79.8 6.0 %copy-start.3 = (bf16[1,896,2048]{2,1,0:T(8,128)(2,1)S(1)}, bf16[1,896,2048]{2,1,0:T(8,128)(2,1)}, u32[]{:S(2)}) copy-start(bf16[1,896,2048]{2,1,0:T(8,128)(2,1)} %param.13) | copy-start | bytes 11010052
  94.0 13.8 %copy-start.6 = (bf16[1024,896]{0,1:T(8,128)(2,1)}, bf16[1024,896]{0,1:T(8,128)(2,1)S(1)}, u32[]{:S(2)}) copy-start(bf16[1024,896]{0,1:T(8,128)(2,1)S(1)} %get-tuple-element.19) | copy-start | bytes 5505028
  124.8 34.9 %copy-start.1 = (s32[256,2]{0,1:T(2,128)S(1)}, s32[256,2]{0,1:T(2,128)}, u32[]{:S(2)}) copy-start(s32[256,2]{0,1:T(2,128)} %param.8) | copy-start | bytes 6148
  159.6 10.2 %copy-start.2 = (f32[2,256]{1,0:T(2,128)}, f32[2,256]{1,0:T(2,128)S(1)}, u32[]{:S(2)}) copy-start(f32[2,256]{1,0:T(2,128)S(1)} %select_reduce_fusion) | copy-start | bytes 6148
where the time goes:
time: 170 us
  Pallas kernels  108 us (64%)
  matrix products  54.9 us (32%)
  local copies, waits for them, and re-layouts  3.64 us (2%)
  other arithmetic  2.46 us (1%)
    pallas_call x1, Pallas kernels, dispatch(): pl.pallas_call(dispatch_kernel(senders, n_rows, capacity, col), out_shape...  66.7 us
    pallas_call x1, Pallas kernels, combine(): pl.pallas_call(combine_kernel(senders, n_rows, capacity, col), out_shape=...  34.4 us
    dot_general x1, matrix products, local(): lax.dot_general(output_rows, w_down, over_cols, preferred_element_type=jn...  8.17 us
    dot_general x1, matrix products, local(): lax.dot_general(hidden, out_scaled, over_rows, preferred_element_type=jnp...  7.81 us
    pallas_call x1, Pallas kernels, router_sum(): pl.pallas_call(body, out_shape=jax.ShapeDtypeStruct(terms.shape[1:], term...  6.74 us
    dot_general x1, matrix products, local(): lax.dot_general(up_back, w_up, over_cols, preferred_element_type=jnp.floa...  6.37 us
    dot_general x1, matrix products, local(): lax.dot_general(token_rows, gate_back, over_rows, preferred_element_type=...  6.02 us
    dot_general x1, matrix products, local(): up_pre = jnp.dot(token_rows, w_up, preferred_element_type=jnp.float32)  6.02 us

commit v1 on v0

v1 whole, which is shorter than its diff:
```python
import math

import jax
import jax.numpy as jnp
from jax import lax
from jax.experimental import pallas as pl
from jax.experimental.pallas import tpu as pltpu
from jax.sharding import PartitionSpec as P

MESH = pl.DeviceIdType.MESH
LANES = 128
CHUNK = 256
BF = jnp.bfloat16
F32 = jnp.float32
NN = (((1,), (0,)), ((), ()))
NT = (((1,), (1,)), ((), ()))
TN = (((0,), (0,)), ((), ()))


def dot(a, b, dims=NN):
    return lax.dot_general(a, b, dims, preferred_element_type=F32)


def remote(src, dst, send, recv, ep, tp):
    return pltpu.make_async_remote_copy(
        src_ref=src,
        dst_ref=dst,
        send_sem=send,
        recv_sem=recv,
        device_id=(ep, tp),
        device_id_type=MESH,
    )


def pair(me, k, size):
    return sum((me // bit + k // bit) % 2 * bit for bit in (1 << b for b in range(size.bit_length() - 1)))


def span(start, size):
    return pl.ds(pl.multiple_of(start * size, size), size)


def each(lo, hi, action):
    def step(k, carry):
        action(k)
        return carry

    lax.fori_loop(lo, hi, step, 0)


def split(value):
    high = value.astype(BF)
    rest = value - high.astype(F32)
    middle = rest.astype(BF)
    low = (rest - middle.astype(F32)).astype(BF)
    return jnp.concatenate([high, middle, low], axis=0)


def layer_kernel(senders, rows, capacity, col, hidden, share):
    seats = 2 * rows
    width = col * seats
    per_chunk = max(1, min(senders, CHUNK // capacity))
    chunk = per_chunk * capacity
    chunks = senders // per_chunk
    half = max(senders // 2, 1)

    def body(tok_ref, cot_ref, routes_ref, router_ref, wg_hbm, wu_hbm, wd_hbm,
             tg_out, mix_out, rt_out, gg, ug, dg,
             wg, wu, wd, pick, tok_send, cot_send, mix_send, mix_in, tok_rows, cot_rows,
             hs, gb, ub, terms, mp_send, mp_got, mix_all, c_buf, y_src, y_buf, fin, home, rt_full, rt_got,
             w_sem, ep_send, ep_recv, y_send, y_recv, c_send, c_recv, m_send, m_recv,
             rc_send, rc_recv, ry_send, ry_recv, h_send, h_recv, p_send, p_recv, t_send, t_recv, r_send, r_recv):
        me = lax.axis_index("ep")
        tp = lax.axis_index("tp")
        row = tp // 2
        core = tp % 2
        partner = row * 2 + (1 - core)
        my_chunk = me // per_chunk

        def seat(step, side):
            return lax.rem(row + step + rows, rows) * 2 + side

        def peer(k):
            return pair(me, k, senders)

        barrier = pltpu.get_barrier_semaphore()
        each(1, senders, lambda k: pl.semaphore_signal(barrier, inc=1, device_id=(peer(k), tp), device_id_type=MESH))
        for k in range(1, seats):
            pl.semaphore_signal(barrier, inc=1, device_id=(me, lax.rem(tp + k, seats)), device_id_type=MESH)

        loads = [pltpu.make_async_copy(src, dst, w_sem.at[i])
                 for i, (src, dst) in enumerate(((wg_hbm, wg), (wu_hbm, wu), (wd_hbm, wd)))]
        for load in loads:
            load.start()

        ids = lax.broadcasted_iota(jnp.int32, (senders, tok_ref.shape[0]), 0)
        is_first = ids == routes_ref[0:1, :]
        is_second = ids == routes_ref[1:2, :]
        member = jnp.where(is_first | is_second, 1.0, 0.0)
        home_rows = tok_ref.shape[0]
        earlier = lax.broadcasted_iota(jnp.int32, (home_rows, home_rows), 0) < lax.broadcasted_iota(
            jnp.int32, (home_rows, home_rows), 1)
        rank = dot(member.astype(BF), jnp.where(earlier, 1.0, 0.0).astype(BF))
        place = jnp.where(member > 0.0, rank, -1.0)
        slot_ids = lax.broadcasted_iota(jnp.int32, (capacity, home_rows), 0).astype(F32)
        for e in range(senders):
            pick[e * capacity:(e + 1) * capacity, :] = jnp.where(slot_ids == place[e:e + 1, :], 1.0, 0.0).astype(BF)

        logits = dot(router_ref[...], tok_ref[...], NT)
        chosen_first = jnp.sum(jnp.where(is_first, logits, 0.0), axis=0, keepdims=True)
        chosen_second = jnp.sum(jnp.where(is_second, logits, 0.0), axis=0, keepdims=True)
        mix_first = 1.0 / (1.0 + jnp.exp(chosen_second - chosen_first))
        mix_second = 1.0 / (1.0 + jnp.exp(chosen_first - chosen_second))
        mix_value = jnp.where(is_first, mix_first, jnp.where(is_second, mix_second, 0.0)).astype(BF)
        for e in range(senders):
            mix_send[e, :, 0:capacity] = dot(mix_value, pick[e * capacity:(e + 1) * capacity, :], NT)
        mix_in[me] = mix_send[me]

        cot_send[...] = dot(pick[...], cot_ref[...]).astype(BF)
        for r in range(rows):
            tok_send[r] = dot(pick[...], tok_ref[:, span(seat(r, core), col)]).astype(BF)
        own = span(me, capacity)
        tok_rows[own, :] = dot(pick[own, :], tok_ref[...]).astype(BF)
        cot_rows[own, span(tp, col)] = cot_send[own, :]

        pl.semaphore_wait(barrier, senders - 1 + seats - 1)

        arrays = (tok_rows, cot_rows)

        def piece(array, block, tp_col):
            return array.at[span(block, capacity), span(tp_col, col)]

        mine = [(1, 0)]
        far = [(1, 0), (0, 0)]
        near = far + [(0, j) for j in range(1, rows)]
        far_hops = [(a, j) for j in range(1, rows) for a in (1, 0)]
        near_hops = [(1, j) for j in range(1, rows)]

        def ep_copy(i, dest, block):
            array, which = near[i]
            source = (tok_send.at[which] if array == 0 else cot_send).at[span(dest, capacity), :]
            return remote(source, piece(arrays[array], block, seat(which, core)),
                          ep_send.at[i, dest], ep_recv.at[i, block], dest, tp)

        def mix_copy(dest, block):
            return remote(mix_send.at[dest], mix_in.at[block], m_send.at[dest], m_recv.at[block], dest, tp)

        def y_copy(array, step, block):
            at = piece(arrays[array], block, tp)
            return remote(at, at, y_send.at[array, step, block], y_recv.at[array, step, block], me, seat(step, core))

        def y_arrival(array, step, block):
            at = piece(arrays[array], block, seat(-step, core))
            return remote(at, at, y_send.at[array, step, block], y_recv.at[array, step, block], me, seat(step, core))

        def c_copy(array, step, block):
            at = piece(arrays[array], block, seat(step, core))
            return remote(at, at, c_send.at[array, step + rows, block], c_recv.at[array, step + rows, block],
                          me, partner)

        def c_arrival(array, step, block):
            at = piece(arrays[array], block, seat(step, 1 - core))
            return remote(at, at, c_send.at[array, step + rows, block], c_recv.at[array, step + rows, block],
                          me, partner)

        def send_to(count):
            def action(k):
                dest = peer(k)
                mix_copy(dest, me).start()
                for i in range(count):
                    ep_copy(i, dest, me).start()

            return action

        each(1, half, send_to(len(near)))
        each(half, senders, send_to(len(far)))

        def spread(block, items, hops):
            for array, step in hops:
                y_copy(array, step, block).start()
            for array, step in items:
                c_copy(array, step, block).start()

        def take(items, hops):
            def action(j):
                block = peer(j)
                for i in range(len(items)):
                    ep_copy(i, block, block).wait_recv()
                spread(block, items, hops)

            return action

        def pass_on(hops):
            def action(j):
                block = peer(j)
                for array, step in hops:
                    y_arrival(array, step, block).wait_recv()
                    c_copy(array, -step, block).start()

            return action

        def settle(items, hops):
            def action(j):
                block = peer(j)
                for array, step in items + [(a, -s) for a, s in hops]:
                    c_arrival(array, step, block).wait_recv()

            return action

        def arrive_mix(j):
            mix_copy(peer(j), peer(j)).wait_recv()

        def home_copy(dest, slot):
            return remote(fin.at[span(dest, capacity), :], home.at[span(slot, capacity), :],
                          h_send.at[dest], h_recv.at[slot], dest, tp)

        def part_copy(dest, slot):
            return remote(mp_send.at[dest], mp_got.at[slot], p_send.at[dest], p_recv.at[slot], dest, tp)

        def rc_copy(step, block):
            return remote(piece(terms, block, seat(step, 1 - core)), c_buf.at[step, span(block, capacity), :],
                          rc_send.at[step, block], rc_recv.at[step, block], me, partner)

        def ry_copy(step, block):
            return remote(y_src.at[step - 1, span(block, capacity), :], y_buf.at[step - 1, span(block, capacity), :],
                          ry_send.at[step, block], ry_recv.at[step, block], me, seat(step, core))

        def start_back(j):
            block = peer(j)
            for step in list(range(1, rows)) + [0]:
                rc_copy(step, block).start()

        def first(j):
            block = peer(j)
            at = span(block, capacity)
            for step in range(1, rows):
                rc_copy(step, block).wait_recv()
                y_src[step - 1, at, :] = (
                    terms[at, span(seat(step, core), col)].astype(F32) + c_buf[step, at, :].astype(F32)
                ).astype(BF)
                ry_copy(step, block).start()

        def second(j):
            block = peer(j)
            at = span(block, capacity)
            rc_copy(0, block).wait_recv()
            value = terms[at, span(tp, col)].astype(F32) + c_buf[0, at, :].astype(F32)
            for step in range(1, rows):
                ry_copy(step, block).wait_recv()
                value = value + y_buf[step - 1, at, :].astype(F32)
            fin[at, :] = value.astype(BF)

            @pl.when(j > 0)
            def _():
                home_copy(block, me).start()

        diagonal = lax.broadcasted_iota(jnp.int32, (capacity, capacity), 0) == lax.broadcasted_iota(
            jnp.int32, (capacity, capacity), 1)

        def to_column(values):
            return jnp.sum(jnp.where(diagonal, values, 0.0), axis=1, keepdims=True)

        def to_row(values):
            return jnp.sum(jnp.where(diagonal, values, 0.0), axis=0, keepdims=True)

        def forward(which):
            at = span(which, chunk)
            mixes = jnp.concatenate(
                [to_column(mix_in[which * per_chunk + i, pl.ds(me, 1), :][:, 0:capacity]) for i in range(per_chunk)],
                axis=0)
            x = tok_rows[at, :]
            dy = cot_rows[at, :]
            total = jnp.zeros((chunk, 1), F32)
            for n0 in range(0, hidden, CHUNK):
                n = min(CHUNK, hidden - n0)
                gate = dot(x, wg[:, n0:n0 + n])
                up = dot(x, wu[:, n0:n0 + n])
                back = dot(dy, wd[n0:n0 + n, :], NT)
                sig = 1.0 / (1.0 + jnp.exp(-gate))
                active = gate * sig
                inner = active * up
                total = total + jnp.sum(inner * back, axis=1, keepdims=True)
                scaled = mixes * back
                gb[at, n0:n0 + n] = (scaled * up * sig * (1.0 + gate * (1.0 - sig))).astype(BF)
                ub[at, n0:n0 + n] = (scaled * active).astype(BF)
                hs[at, n0:n0 + n] = (mixes * inner).astype(BF)
            for i in range(per_chunk):
                line = to_row(total[i * capacity:(i + 1) * capacity, :])
                mp_send[which * per_chunk + i, :, 0:capacity] = jnp.broadcast_to(line, (8, capacity))

        def backward(which):
            at = span(which, chunk)
            gate_back = gb[at, :]
            up_back = ub[at, :]
            for d0 in range(0, width, 512):
                terms[at, d0:d0 + 512] = (
                    dot(gate_back, wg[d0:d0 + 512, :], NT) + dot(up_back, wu[d0:d0 + 512, :], NT)
                ).astype(BF)

        def order(s):
            if chunks != 4:
                return s
            return pair(s, s // 2 * ((my_chunk + my_chunk // 2) % 2), chunks)

        spread(me, mine, near_hops)

        def step_of(s):
            k = order(s)
            lo = k * per_chunk
            hi = lo + per_chunk
            near_lo, near_hi = jnp.maximum(lo, 1), jnp.minimum(hi, half)
            far_lo = jnp.maximum(lo, half)
            own_hi = jnp.where(s == 0, 1, 0)
            each(near_lo, near_hi, take(near, near_hops))
            each(far_lo, hi, take(far, far_hops))

            @pl.when(s > 0)
            def _():
                before = order(s - 1) * per_chunk
                each(before, before + per_chunk, second)

            each(0, own_hi, pass_on(near_hops))
            each(near_lo, near_hi, pass_on(near_hops))
            each(far_lo, hi, pass_on(far_hops))
            each(0, own_hi, settle(mine, near_hops))
            each(near_lo, near_hi, settle(near, near_hops))
            each(far_lo, hi, settle(far, far_hops))
            each(jnp.maximum(lo, 1), hi, arrive_mix)

            @pl.when(s == 0)
            def _():
                for load in loads:
                    load.wait()

            which = pair(my_chunk, k, chunks)
            forward(which)
            each(jnp.maximum(lo, 1), hi, lambda j: part_copy(peer(j), me).start())
            backward(which)
            each(lo, hi, start_back)
            each(lo, hi, first)

        each(0, chunks, step_of)
        mp_got[me] = mp_send[me]

        def gate_up(i):
            at = span(i, CHUNK)
            x = tok_rows[:, at]
            gg[at, :] = dot(x, gb[...], TN).astype(BF)
            ug[at, :] = dot(x, ub[...], TN).astype(BF)

        def down(i):
            at = span(i, LANES)
            dg[at, :] = dot(hs[:, at], cot_rows[...], TN).astype(BF)

        parts = width // CHUNK
        last = order(chunks - 1) * per_chunk
        middle = last + (per_chunk + 1) // 2
        each(0, parts // 2, gate_up)
        each(last, middle, second)
        each(parts // 2, parts * 3 // 4, gate_up)
        each(middle, last + per_chunk, second)
        each(parts * 3 // 4, parts, gate_up)

        each(1, senders, lambda j: part_copy(peer(j), peer(j)).wait_recv())
        mix_all[0] = mp_got[...]

        def t_copy(k):
            return remote(mp_got, mix_all.at[k], t_send.at[k], t_recv.at[k], me, lax.rem(tp + k, seats))

        for k in range(1, seats):
            t_copy(k).start()
        down_parts = hidden // LANES
        each(0, (down_parts + 1) // 2, down)
        for k in range(1, seats):
            t_copy(k).wait()

        slot_mix = jnp.sum(mix_all[...], axis=0)
        grads = []
        for e in range(senders):
            column = to_column(slot_mix[e, 0:1, 0:capacity])
            chosen = pick[e * capacity:(e + 1) * capacity, :].astype(F32)
            grads.append(jnp.sum(column * chosen, axis=0, keepdims=True))
        grads = jnp.concatenate(grads, axis=0)
        mg_first = jnp.sum(jnp.where(is_first, grads, 0.0), axis=0, keepdims=True)
        mg_second = jnp.sum(jnp.where(is_second, grads, 0.0), axis=0, keepdims=True)
        mix_out[0:1, :] = mg_first
        mix_out[1:2, :] = mg_second
        lg_first = mix_first * mix_second * (mg_first - mg_second)
        route_grad = split(jnp.where(is_first, lg_first, jnp.where(is_second, -lg_first, 0.0)))
        raw = dot(route_grad, tok_ref[...])
        norm_scale = 1.0 / math.sqrt(home_rows * senders)
        rt_full[...] = (raw[0:senders] + raw[senders:2 * senders] + raw[2 * senders:]) * norm_scale

        def rt_cols(dest):
            return span((dest * seats + tp) * share // LANES, LANES)

        def r_copy(dest, slot):
            return remote(rt_full.at[:, rt_cols(dest)], rt_got.at[slot], r_send.at[dest], r_recv.at[slot], dest, tp)

        each(1, senders, lambda k: r_copy(peer(k), me).start())
        rt_got[me] = rt_full[:, rt_cols(me)]
        each((down_parts + 1) // 2, down_parts, down)

        home[own, :] = fin[own, :]
        each(1, senders, lambda k: home_copy(peer(k), peer(k)).wait_recv())
        cols = router_ref[:, span(tp, col)]
        tg_out[...] = (
            dot(pick[...], home[...], TN) + dot(route_grad, jnp.concatenate([cols, cols, cols], axis=0), TN)
        ).astype(BF)
        each(1, senders, lambda k: r_copy(peer(k), peer(k)).wait_recv())
        rt_out[...] = jnp.sum(rt_got[...], axis=0)

        def close(items, hops):
            def action(j):
                block = peer(j)
                for array, step in items + [(a, -s) for a, s in hops]:
                    c_copy(array, step, block).wait_send()
                for array, step in hops:
                    y_copy(array, step, block).wait_send()

            return action

        close(mine, near_hops)(0)
        each(1, half, close(near, near_hops))
        each(half, senders, close(far, far_hops))

        def close_back(j):
            block = peer(j)
            for step in range(rows):
                rc_copy(step, block).wait_send()
            for step in range(1, rows):
                ry_copy(step, block).wait_send()

        each(0, senders, close_back)

        def close_sends(count):
            def action(k):
                dest = peer(k)
                for i in range(count):
                    ep_copy(i, dest, me).wait_send()
                mix_copy(dest, me).wait_send()
                part_copy(dest, me).wait_send()
                home_copy(dest, me).wait_send()
                r_copy(dest, me).wait_send()

            return action

        each(1, half, close_sends(len(near)))
        each(half, senders, close_sends(len(far)))

    return body


def layer(tokens, cotangent, routes, router, w_gate, w_up, w_down):
    home_rows, width = tokens.shape
    senders = router.shape[0]
    seats = lax.axis_size("tp")
    rows = seats // 2
    col = width // seats
    hidden = w_gate.shape[1]
    capacity = home_rows * routes.shape[0] * 2 // senders
    slots = senders * capacity
    share = width // (senders * seats)
    vmem = pl.BlockSpec(memory_space=pltpu.VMEM)
    hbm = pl.BlockSpec(memory_space=pl.ANY)
    dma = pltpu.SemaphoreType.DMA

    def buf(shape, dtype=BF):
        return pltpu.VMEM(shape, dtype)

    return pl.pallas_call(
        layer_kernel(senders, rows, capacity, col, hidden, share),
        out_shape=(
            jax.ShapeDtypeStruct((home_rows, col), BF),
            jax.ShapeDtypeStruct((2, home_rows), F32),
            jax.ShapeDtypeStruct((senders, LANES), F32),
            jax.ShapeDtypeStruct((width, hidden), BF),
            jax.ShapeDtypeStruct((width, hidden), BF),
            jax.ShapeDtypeStruct((hidden, width), BF),
        ),
        in_specs=[vmem] * 4 + [hbm] * 3,
        out_specs=[vmem] * 6,
        scratch_shapes=[
            buf((width, hidden)), buf((width, hidden)), buf((hidden, width)),
            buf((slots, home_rows)), buf((rows, slots, col)), buf((slots, col)),
            buf((senders, senders, LANES), F32), buf((senders, senders, LANES), F32),
            buf((slots, width)), buf((slots, width)),
            buf((slots, hidden)), buf((slots, hidden)), buf((slots, hidden)), buf((slots, width)),
            buf((senders, 8, LANES), F32), buf((senders, 8, LANES), F32), buf((seats, senders, 8, LANES), F32),
            buf((rows, slots, col)), buf((rows - 1, slots, col)), buf((rows - 1, slots, col)),
            buf((slots, col)), buf((slots, col)),
            buf((senders, width), F32), buf((senders, senders, LANES), F32),
            dma((3,)),
            dma((1 + rows, senders)), dma((1 + rows, senders)),
            dma((2, rows, senders)), dma((2, rows, senders)),
            dma((2, 2 * rows, senders)), dma((2, 2 * rows, senders)),
            dma((senders,)), dma((senders,)),
            dma((rows, senders)), dma((rows, senders)),
            dma((rows, senders)), dma((rows, senders)),
            dma((senders,)), dma((senders,)),
            dma((senders,)), dma((senders,)),
            dma((seats,)), dma((seats,)),
            dma((senders,)), dma((senders,)),
        ],
        compiler_params=pltpu.CompilerParams(has_side_effects=True, collective_id=0, vmem_limit_bytes=60 << 20),
        name="layer",
    )(tokens, cotangent, routes, router, w_gate, w_up, w_down)


def local(tokens, routes, router_matrix, cotangent, gate_proj, up_proj, down_proj):
    ep_size = lax.axis_size("ep")
    tp_size = lax.axis_size("tp")
    token_grad, mixing, router_rows, gate_grad, up_grad, down_grad = layer(
        tokens, cotangent, routes.T, router_matrix.T, gate_proj[0], up_proj[0], down_proj[0]
    )
    share = tokens.shape[1] // (ep_size * tp_size)
    start = (lax.axis_index("ep") * tp_size + lax.axis_index("tp")) * share % LANES
    router_grad = lax.dynamic_slice_in_dim(router_rows, start, share, 1).T
    return (token_grad, mixing.T, router_grad, gate_grad[None], up_grad[None], down_grad[None])


def solution(mesh):
    return jax.shard_map(
        local,
        mesh=mesh,
        in_specs=(
            P("ep", None),
            P("ep", None),
            P(),
            P("ep", "tp"),
            P("ep", None, "tp"),
            P("ep", None, "tp"),
            P("ep", "tp", None),
        ),
        out_specs=(
            P("ep", "tp"),
            P("ep", None),
            P(("ep", "tp"), None),
            P("ep", None, "tp"),
            P("ep", None, "tp"),
            P("ep", "tp", None),
        ),
        check_vma=False,
    )
```

time: 170 us -> 150 us (0.88)
  matrix products: 54.9 us -> 0 us
  Pallas kernels: 108 us -> 136 us
  local copies, waits for them, and re-layouts: 3.64 us -> 13.8 us
  other arithmetic: 2.46 us -> 0 us
    dot_general x15 -> x0, matrix products: 54.9 us -> none  [the longest x1 8.17 us: local(): lax.dot_general(output_rows, w_down, over_cols, preferred_element_type=jn...]
    pallas_call x3 -> x1, Pallas kernels: 108 us -> 136 us  [layer(): pl.pallas_call(layer_kernel(senders, rows, capacity, col, hidden, share),...]
    unnamed x16 -> x9, local copies, waits for them, and re-layouts: 2.34 us -> 12.4 us
where the time goes in v1:
time: 150 us
  Pallas kernels  136 us (91%)
  local copies, waits for them, and re-layouts  13.8 us (9%)
    pallas_call x1, Pallas kernels, layer(): pl.pallas_call(layer_kernel(senders, rows, capacity, col, hidden, share),...  136 us
    unnamed x9, local copies, waits for them, and re-layouts  12.4 us

profile of v1, /device:TPU:0, one launch (start us, length us, event | category | flops | bytes accessed | tf_op | source)
XLA Modules:
  0.0 150.1 jit_solution(13331442511467195391)
XLA Ops:
  0.7 135.7 %layer.1 = (bf16[256,512]{1,0:T(8,128)(2,1)}, f32[2,256]{1,0:T(2,128)}, f32[8,128]{1,0:T(8,128)}, bf16[2048,896]{1,0:T(8,128)(2,1)}, bf16[2048,896]{1,0:T(8,128)(2,1)}, /*index=5*/bf16[896,2048]{1,0:T(8,128)(2,1)}) custom-call(bf16[256,2048]{1,0:T(8,128)(2,1)} %tok_ref.1, bf16[256,512]{1,0:T(8,128)(2,1)} %cot_ref.1, s32[2,256]{1,0:T(2,128)} %bitcast.18, ...), custom_call_target="tpu_custom_call" | custom-call | tf_op jit(solution)/shard_map/layer/pallas_call | solution.py:471
  136.4 1.3 dynamic-slice_bitcast_fusion
  137.7 1.7 %copy.18 = bf16[256,512]{1,0:T(8,128)(2,1)} copy(bf16[256,512]{1,0:T(8,128)(2,1)} %get-tuple-element.24) | data formatting | bytes 524288
  139.4 1.3 copy.19
  140.6 0.0 copy-start.1
  140.6 4.3 %copy.20 = bf16[1,2048,896]{2,1,0:T(8,128)(2,1)} copy(bf16[1,2048,896]{2,1,0:T(8,128)(2,1)} %bitcast.13) | data formatting | bytes 7340032
  144.9 0.0 copy-done.1
  144.9 0.0 copy-start
  144.9 1.9 %copy.21 = bf16[1,2048,896]{2,1,0:T(8,128)(2,1)} copy(bf16[1,2048,896]{2,1,0:T(8,128)(2,1)S(1)} %bitcast.12) | data formatting | bytes 7340032
  146.8 1.5 copy-done
  148.3 1.8 %copy.22 = bf16[1,896,2048]{2,1,0:T(8,128)(2,1)} copy(bf16[1,896,2048]{2,1,0:T(8,128)(2,1)S(1)} %bitcast.11) | data formatting | bytes 7340032
Async XLA Ops:
  140.6 4.3 %copy-start.1 = (bf16[2048,896]{1,0:T(8,128)(2,1)S(1)}, bf16[2048,896]{1,0:T(8,128)(2,1)}, u32[]{:S(2)}) copy-start(bf16[2048,896]{1,0:T(8,128)(2,1)} %get-tuple-element.16) | copy-start | bytes 11010052
  144.9 3.4 %copy-start = (bf16[896,2048]{1,0:T(8,128)(2,1)S(1)}, bf16[896,2048]{1,0:T(8,128)(2,1)}, u32[]{:S(2)}) copy-start(bf16[896,2048]{1,0:T(8,128)(2,1)} %get-tuple-element.17) | copy-start | bytes 11010052

commit v2 on v1

v2 whole, which is shorter than its diff:
```python
import math

import jax
import jax.numpy as jnp
from jax import lax
from jax.experimental import pallas as pl
from jax.experimental.pallas import tpu as pltpu
from jax.sharding import PartitionSpec as P

MESH = pl.DeviceIdType.MESH
LANES = 128
CHUNK = 256
OUTER_TAKES = (2, 4, 4, 4, 4, 6, 7, 8, 8, 8, 8, 8, 8, 8, 8, 8, 8)
INNER_TAKES = (2, 4, 4, 4, 4, 7, 8, 8, 8, 8, 8, 8, 8, 8, 8, 8, 8)
BF = jnp.bfloat16
F32 = jnp.float32
NN = (((1,), (0,)), ((), ()))
NT = (((1,), (1,)), ((), ()))
TN = (((0,), (0,)), ((), ()))


def dot(a, b, dims=NN):
    return lax.dot_general(a, b, dims, preferred_element_type=F32)


def remote(src, dst, send, recv, ep, tp):
    return pltpu.make_async_remote_copy(
        src_ref=src,
        dst_ref=dst,
        send_sem=send,
        recv_sem=recv,
        device_id=(ep, tp),
        device_id_type=MESH,
    )


def pair(me, k, size):
    return sum((me // bit + k // bit) % 2 * bit for bit in (1 << b for b in range(size.bit_length() - 1)))


def span(start, size):
    return pl.ds(pl.multiple_of(start * size, size), size)


def each(lo, hi, action):
    def step(k, carry):
        action(k)
        return carry

    lax.fori_loop(lo, hi, step, 0)


def split(value):
    high = value.astype(BF)
    rest = value - high.astype(F32)
    middle = rest.astype(BF)
    low = (rest - middle.astype(F32)).astype(BF)
    return jnp.concatenate([high, middle, low], axis=0)


def layer_kernel(senders, rows, capacity, col, hidden, share):
    seats = 2 * rows
    width = col * seats
    per_chunk = max(1, min(senders, CHUNK // capacity))
    chunk = per_chunk * capacity
    chunks = senders // per_chunk
    half = max(senders // 2, 1)

    def body(tok_hbm, cot_hbm, routes_hbm, router_hbm, wg_hbm, wu_hbm, wd_hbm,
             tg_out, mix_out, rt_out, gg, ug, dg,
             tok_ref, cot_ref, routes_ref, router_ref, wg, wu, wd, pick, tok_send, cot_send, cot_raw, cot_more, mix_send, mix_in, tok_rows, cot_rows,
             hs, gb, ub, terms, mp_send, mp_got, mix_all, c_buf, y_buf, home, rt_full, rt_got,
             w_sem, raw_send, raw_recv, ep_send, ep_recv, y_send, y_recv, c_send, c_recv, m_send, m_recv,
             rc_send, rc_recv, ry_send, ry_recv, h_send, h_recv, p_send, p_recv, t_send, t_recv, r_send, r_recv):
        me = lax.axis_index("ep")
        tp = lax.axis_index("tp")
        row = tp // 2
        core = tp % 2
        partner = row * 2 + (1 - core)
        my_chunk = me // per_chunk

        def seat(step, side):
            return lax.rem(row + step + rows, rows) * 2 + side

        def peer(k):
            return pair(me, k, senders)

        def raw_copy(step):
            return remote(cot_ref, cot_raw.at[step - 1], raw_send.at[step], raw_recv.at[step], me, seat(step, core))

        barrier = pltpu.get_barrier_semaphore()
        each(1, senders, lambda k: pl.semaphore_signal(barrier, inc=1, device_id=(peer(k), tp), device_id_type=MESH))
        for k in range(1, seats):
            pl.semaphore_signal(barrier, inc=1, device_id=(me, lax.rem(tp + k, seats)), device_id_type=MESH)

        loads = [pltpu.make_async_copy(src, dst, w_sem.at[i])
                 for i, (src, dst) in enumerate((
                     (routes_hbm, routes_ref), (tok_hbm, tok_ref), (router_hbm, router_ref), (cot_hbm, cot_ref),
                     (wg_hbm, wg), (wu_hbm, wu), (wd_hbm, wd)))]
        for load in loads:
            load.start()
        loads[0].wait()
        loads[3].wait()
        pl.semaphore_wait(barrier, senders - 1 + seats - 1)
        for step in range(1, rows):
            raw_copy(step).start()

        ids = lax.broadcasted_iota(jnp.int32, (senders, tok_ref.shape[0]), 0)
        is_first = ids == routes_ref[0:1, :]
        is_second = ids == routes_ref[1:2, :]
        member = jnp.where(is_first | is_second, 1.0, 0.0)
        home_rows = tok_ref.shape[0]
        earlier = lax.broadcasted_iota(jnp.int32, (home_rows, home_rows), 0) < lax.broadcasted_iota(
            jnp.int32, (home_rows, home_rows), 1)
        rank = dot(member.astype(BF), jnp.where(earlier, 1.0, 0.0).astype(BF))
        place = jnp.where(member > 0.0, rank, -1.0)
        slot_ids = lax.broadcasted_iota(jnp.int32, (capacity, home_rows), 0).astype(F32)
        for e in range(senders):
            pick[e * capacity:(e + 1) * capacity, :] = jnp.where(slot_ids == place[e:e + 1, :], 1.0, 0.0).astype(BF)

        loads[1].wait()

        def choose_rows(i):
            at = span(i, CHUNK)
            cot_send[at, :] = dot(pick[at, :], cot_ref[...]).astype(BF)
            for r in range(rows):
                tok_send[r, at, :] = dot(pick[at, :], tok_ref[:, span(seat(r, core), col)]).astype(BF)

        each(0, senders * capacity // CHUNK, choose_rows)
        own = span(me, capacity)
        tok_rows[own, :] = dot(pick[own, :], tok_ref[...]).astype(BF)
        cot_rows[own, span(tp, col)] = cot_send[own, :]

        arrays = (tok_rows, cot_rows)

        def piece(array, block, tp_col):
            return array.at[span(block, capacity), span(tp_col, col)]

        mine = [(1, -j) for j in range(rows)]
        far = [(1, 0), (0, 0)]
        early = far + [(0, j) for j in range(1, rows)]
        near = early + [(1, -j) for j in range(1, rows)]
        far_hops = [(a, j) for j in range(1, rows) for a in (1, 0)]
        near_first = me // half * half

        def ep_copy(i, dest, block):
            array, which = near[i]
            if array == 1 and which < 0:
                source = cot_more.at[-which - 1, span(dest - near_first, capacity), :]
            else:
                source = (tok_send.at[which] if array == 0 else cot_send).at[span(dest, capacity), :]
            return remote(source, piece(arrays[array], block, seat(which, core)),
                          ep_send.at[i, dest], ep_recv.at[i, block], dest, tp)

        def mix_copy(dest, block):
            return remote(mix_send.at[dest], mix_in.at[block], m_send.at[dest], m_recv.at[block], dest, tp)

        def y_copy(array, step, block):
            at = piece(arrays[array], block, tp)
            return remote(at, at, y_send.at[array, step, block], y_recv.at[array, step, block], me, seat(step, core))

        def y_arrival(array, step, block):
            at = piece(arrays[array], block, seat(-step, core))
            return remote(at, at, y_send.at[array, step, block], y_recv.at[array, step, block], me, seat(step, core))

        def c_copy(array, step, block):
            at = piece(arrays[array], block, seat(step, core))
            return remote(at, at, c_send.at[array, step + rows, block], c_recv.at[array, step + rows, block],
                          me, partner)

        def c_arrival(array, step, block):
            at = piece(arrays[array], block, seat(step, 1 - core))
            return remote(at, at, c_send.at[array, step + rows, block], c_recv.at[array, step + rows, block],
                          me, partner)

        inner = (my_chunk + my_chunk // 2) % 2

        def choose(s, values):
            return sum(jnp.where(s == i, v, 0) for i, v in enumerate(values))

        def order(s):
            if chunks != 4:
                return s
            return jnp.where(inner == 1, choose(s, (3, 1, 0, 2)), choose(s, (0, 2, 1, 3)))

        def send(lo, hi):
            def action(k):
                for i in range(lo, hi):
                    ep_copy(i, peer(k), me).start()

            return action

        def send_far(on):
            flip = inner if chunks == 4 else 0
            for s in range(half // per_chunk, chunks):
                start = pair(s, flip, chunks) * per_chunk
                each(start, start + per_chunk * on, send(0, len(far)))

        c_copy(1, 0, me).start()
        each(1, half, send(0, len(early)))
        loads[2].wait()
        logits = dot(router_ref[...], tok_ref[...], NT)
        chosen_first = jnp.sum(jnp.where(is_first, logits, 0.0), axis=0, keepdims=True)
        chosen_second = jnp.sum(jnp.where(is_second, logits, 0.0), axis=0, keepdims=True)
        mix_first = 1.0 / (1.0 + jnp.exp(chosen_second - chosen_first))
        mix_second = 1.0 / (1.0 + jnp.exp(chosen_first - chosen_second))
        mix_value = jnp.where(is_first, mix_first, jnp.where(is_second, mix_second, 0.0)).astype(BF)
        for e in range(senders):
            mix_send[e, :, 0:capacity] = dot(mix_value, pick[e * capacity:(e + 1) * capacity, :], NT)
        mix_in[me] = mix_send[me]
        each(1, senders, lambda k: mix_copy(peer(k), me).start())
        send_far(inner)
        for step in range(1, rows):
            raw_copy(step).wait_recv()
            for n0 in range(0, half * capacity, CHUNK):
                cot_more[step - 1, n0:n0 + CHUNK, :] = dot(
                    pick[pl.ds(pl.multiple_of(near_first * capacity + n0, capacity), CHUNK), :], cot_raw[step - 1]
                ).astype(BF)
            cot_rows[own, span(seat(-step, core), col)] = cot_more[step - 1, span(me - near_first, capacity), :]
            c_copy(1, -step, me).start()
        each(1, half, send(len(early), len(near)))
        send_far(1 - inner)

        def take(items, hops):
            def action(j):
                block = peer(j)
                for i, (array, step) in enumerate(items):
                    ep_copy(i, block, block).wait_recv()
                    for a, hop in hops:
                        if a == array and step == 0:
                            y_copy(array, hop, block).start()
                    c_copy(array, step, block).start()

            return action

        def pass_on(hops):
            def action(j):
                block = peer(j)
                for array, step in hops:
                    y_arrival(array, step, block).wait_recv()
                    c_copy(array, -step, block).start()

            return action

        def settle(items, hops):
            def action(j):
                block = peer(j)
                for array, step in items + [(a, -s) for a, s in hops]:
                    c_arrival(array, step, block).wait_recv()

            return action

        def arrive_mix(j):
            mix_copy(peer(j), peer(j)).wait_recv()

        def home_copy(dest, slot):
            return remote(piece(terms, dest, tp), home.at[span(slot, capacity), :],
                          h_send.at[dest], h_recv.at[slot], dest, tp)

        def part_copy(dest, slot):
            return remote(mp_send.at[dest], mp_got.at[slot], p_send.at[dest], p_recv.at[slot], dest, tp)

        def rc_copy(step, block):
            return remote(piece(terms, block, seat(step, 1 - core)), c_buf.at[step, span(block, capacity), :],
                          rc_send.at[step, block], rc_recv.at[step, block], me, partner)

        def ry_copy(step, block):
            return remote(piece(terms, block, seat(step, core)), y_buf.at[step - 1, span(block, capacity), :],
                          ry_send.at[step, block], ry_recv.at[step, block], me, seat(step, core))

        def start_back(j):
            block = peer(j)
            for step in range(1, rows):
                rc_copy(step, block).start()

        def rest_back(j):
            rc_copy(0, peer(j)).start()

        def first(j):
            block = peer(j)
            at = span(block, capacity)
            for step in range(1, rows):
                rc_copy(step, block).wait_recv()
                cols = span(seat(step, core), col)
                terms[at, cols] = (terms[at, cols].astype(F32) + c_buf[step, at, :].astype(F32)).astype(BF)
                ry_copy(step, block).start()

        def second(j):
            block = peer(j)
            at = span(block, capacity)
            rc_copy(0, block).wait_recv()
            value = terms[at, span(tp, col)].astype(F32) + c_buf[0, at, :].astype(F32)
            for step in range(1, rows):
                ry_copy(step, block).wait_recv()
                value = value + y_buf[step - 1, at, :].astype(F32)
            terms[at, span(tp, col)] = value.astype(BF)

            @pl.when(j > 0)
            def _():
                home_copy(block, me).start()

        diagonal = lax.broadcasted_iota(jnp.int32, (capacity, capacity), 0) == lax.broadcasted_iota(
            jnp.int32, (capacity, capacity), 1)

        def to_column(values):
            return jnp.sum(jnp.where(diagonal, values, 0.0), axis=1, keepdims=True)

        def to_row(values):
            return jnp.sum(jnp.where(diagonal, values, 0.0), axis=0, keepdims=True)

        def forward(which):
            at = span(which, chunk)
            mixes = jnp.concatenate(
                [to_column(mix_in[which * per_chunk + i, pl.ds(me, 1), :][:, 0:capacity]) for i in range(per_chunk)],
                axis=0)
            x = tok_rows[at, :]
            dy = cot_rows[at, :]
            total = jnp.zeros((chunk, 1), F32)
            for n0 in range(0, hidden, CHUNK):
                n = min(CHUNK, hidden - n0)
                gate = dot(x, wg[:, n0:n0 + n])
                up = dot(x, wu[:, n0:n0 + n])
                back = dot(dy, wd[n0:n0 + n, :], NT)
                sig = 1.0 / (1.0 + jnp.exp(-gate))
                active = gate * sig
                inner = active * up
                total = total + jnp.sum(inner * back, axis=1, keepdims=True)
                scaled = mixes * back
                gb[at, n0:n0 + n] = (scaled * up * sig * (1.0 + gate * (1.0 - sig))).astype(BF)
                ub[at, n0:n0 + n] = (scaled * active).astype(BF)
                hs[at, n0:n0 + n] = (mixes * inner).astype(BF)
            for i in range(per_chunk):
                line = to_row(total[i * capacity:(i + 1) * capacity, :])
                mp_send[which * per_chunk + i, :, 0:capacity] = jnp.broadcast_to(line, (8, capacity))

        def backward(which):
            at = span(which, chunk)
            gate_back = gb[at, :]
            up_back = ub[at, :]
            for d0 in range(0, width, 512):
                terms[at, d0:d0 + 512] = (
                    dot(gate_back, wg[d0:d0 + 512, :], NT) + dot(up_back, wu[d0:d0 + 512, :], NT)
                ).astype(BF)

        def ranged(own_action, near_action, far_action):
            def run(lo, hi):
                if own_action is not None:
                    each(lo, jnp.minimum(hi, 1), own_action)
                each(jnp.maximum(lo, 1), jnp.minimum(hi, half), near_action)
                each(jnp.maximum(lo, half), hi, far_action)

            return run

        take_range = ranged(None, take(near, []), take(far, far_hops))
        settle_range = ranged(settle(mine, []), settle(near, []), settle(far, far_hops))
        part = (per_chunk + 1) // 2

        def take_halves(lo, hi):
            def one(h):
                start = order(h // 2) * per_chunk + h % 2 * part
                take_range(start, start + part)

            each(lo, hi, one)

        def taken(s, point):
            def of(table):
                return choose(s, [table[4 * i + point] for i in range(4)])

            return jnp.where(inner == 1, of(INNER_TAKES), of(OUTER_TAKES))

        def take_point(s, point):
            take_halves(taken(s, point - 1), taken(s, point))

        take_halves(0, 2)

        def halves(first_step):
            return [span(pair(my_chunk, order(s), chunks), chunk) for s in range(first_step, first_step + chunks // 2)]

        def joined(ref, first_step, cols):
            return jnp.concatenate([ref[at, cols] for at in halves(first_step)], axis=0)

        def gate_up_early(i):
            at = span(i, CHUNK)
            x = joined(tok_rows, 0, at)
            gg[at, :] = dot(x, joined(gb, 0, slice(None)), TN).astype(BF)
            ug[at, :] = dot(x, joined(ub, 0, slice(None)), TN).astype(BF)

        def gate_up(i):
            at = span(i, CHUNK)
            x = joined(tok_rows, chunks // 2, at)
            gg[at, :] = (gg[at, :].astype(F32) + dot(x, joined(gb, chunks // 2, slice(None)), TN)).astype(BF)
            ug[at, :] = (ug[at, :].astype(F32) + dot(x, joined(ub, chunks // 2, slice(None)), TN)).astype(BF)

        def step_of(s):
            lo = order(s) * per_chunk
            hi = lo + per_chunk
            before = order(jnp.maximum(s - 1, 0)) * per_chunk
            earlier_chunk = order(jnp.maximum(s - 2, 0)) * per_chunk
            which = pair(my_chunk, order(s), chunks)

            each(jnp.maximum(lo, half), hi, pass_on(far_hops))
            settle_range(lo, hi)
            each(jnp.maximum(lo, 1), hi, arrive_mix)

            @pl.when(s == 0)
            def _():
                for load in loads[4:]:
                    load.wait()

            forward(which)
            each(jnp.maximum(lo, 1), hi, lambda j: part_copy(peer(j), me).start())
            take_point(s, 1)
            each(earlier_chunk, earlier_chunk + jnp.where(s > 1, per_chunk, 0), second)
            backward(which)
            each(lo, hi, start_back)
            each(lo, hi, rest_back)
            take_point(s, 2)
            each(0, jnp.where(s == chunks // 2 - 1, width // CHUNK, 0), gate_up_early)
            take_point(s, 3)
            each(before, before + jnp.where(s == chunks - 1, per_chunk, 0), second)
            each(lo, hi, first)
            take_point(s, 4)

        each(0, chunks, step_of)
        mp_got[me] = mp_send[me]

        def down(i):
            at = span(i, LANES)
            for n0 in range(0, width, 512):
                dg[at, n0:n0 + 512] = dot(hs[:, at], cot_rows[:, n0:n0 + 512], TN).astype(BF)

        parts = width // CHUNK
        last = order(chunks - 1) * per_chunk
        middle = last + (per_chunk + 1) // 2
        each(0, parts // 2, gate_up)
        each(last, middle, second)
        each(parts // 2, parts * 3 // 4, gate_up)
        each(middle, last + per_chunk, second)
        each(parts * 3 // 4, parts, gate_up)

        each(1, senders, lambda j: part_copy(peer(j), peer(j)).wait_recv())
        mix_all[0] = mp_got[...]

        def t_copy(k):
            return remote(mp_got, mix_all.at[k], t_send.at[k], t_recv.at[k], me, lax.rem(tp + k, seats))

        for k in range(1, seats):
            t_copy(k).start()
        down_parts = hidden // LANES
        each(0, (down_parts + 1) // 2, down)
        for k in range(1, seats):
            t_copy(k).wait()

        slot_mix = jnp.sum(mix_all[...], axis=0)
        grads = []
        for e in range(senders):
            column = to_column(slot_mix[e, 0:1, 0:capacity])
            chosen = pick[e * capacity:(e + 1) * capacity, :].astype(F32)
            grads.append(jnp.sum(column * chosen, axis=0, keepdims=True))
        grads = jnp.concatenate(grads, axis=0)
        mg_first = jnp.sum(jnp.where(is_first, grads, 0.0), axis=0, keepdims=True)
        mg_second = jnp.sum(jnp.where(is_second, grads, 0.0), axis=0, keepdims=True)
        mix_out[0:1, :] = mg_first
        mix_out[1:2, :] = mg_second
        lg_first = mix_first * mix_second * (mg_first - mg_second)
        route_grad = split(jnp.where(is_first, lg_first, jnp.where(is_second, -lg_first, 0.0)))
        raw = dot(route_grad, tok_ref[...])
        norm_scale = 1.0 / math.sqrt(home_rows * senders)
        rt_full[...] = (raw[0:senders] + raw[senders:2 * senders] + raw[2 * senders:]) * norm_scale

        def rt_cols(dest):
            return span((dest * seats + tp) * share // LANES, LANES)

        def r_copy(dest, slot):
            return remote(rt_full.at[:, rt_cols(dest)], rt_got.at[slot], r_send.at[dest], r_recv.at[slot], dest, tp)

        each(1, senders, lambda k: r_copy(peer(k), me).start())
        rt_got[me] = rt_full[:, rt_cols(me)]
        each((down_parts + 1) // 2, down_parts, down)

        def close(items, hops):
            def action(j):
                block = peer(j)
                for array, step in items + [(a, -s) for a, s in hops]:
                    c_copy(array, step, block).wait_send()
                for array, step in hops:
                    y_copy(array, step, block).wait_send()

            return action

        for step in range(1, rows):
            raw_copy(step).wait_send()
        close(mine, [])(0)
        each(1, half, close(near, []))
        each(half, senders, close(far, far_hops))

        def close_back(j):
            block = peer(j)
            for step in range(rows):
                rc_copy(step, block).wait_send()
            for step in range(1, rows):
                ry_copy(step, block).wait_send()

        each(0, senders, close_back)

        def close_dispatch(count):
            def action(k):
                dest = peer(k)
                for i in range(count):
                    ep_copy(i, dest, me).wait_send()
                mix_copy(dest, me).wait_send()

            return action

        each(1, half, close_dispatch(len(near)))
        each(half, senders, close_dispatch(len(far)))

        home[own, :] = terms[own, span(tp, col)]
        each(1, senders, lambda k: home_copy(peer(k), peer(k)).wait_recv())
        cols = router_ref[:, span(tp, col)]
        tg_out[...] = (
            dot(pick[...], home[...], TN) + dot(route_grad, jnp.concatenate([cols, cols, cols], axis=0), TN)
        ).astype(BF)
        each(1, senders, lambda k: r_copy(peer(k), peer(k)).wait_recv())
        rt_out[...] = jnp.sum(rt_got[...], axis=0)

        def close_sends(dest):
            part_copy(dest, me).wait_send()
            home_copy(dest, me).wait_send()
            r_copy(dest, me).wait_send()

        each(1, senders, lambda k: close_sends(peer(k)))

    return body


def layer(tokens, cotangent, routes, router, w_gate, w_up, w_down):
    home_rows, width = tokens.shape
    senders = router.shape[0]
    seats = lax.axis_size("tp")
    rows = seats // 2
    col = width // seats
    hidden = w_gate.shape[1]
    capacity = home_rows * routes.shape[0] * 2 // senders
    slots = senders * capacity
    share = width // (senders * seats)
    vmem = pl.BlockSpec(memory_space=pltpu.VMEM)
    hbm = pl.BlockSpec(memory_space=pltpu.HBM)
    dma = pltpu.SemaphoreType.DMA

    def buf(shape, dtype=BF):
        return pltpu.VMEM(shape, dtype)

    return pl.pallas_call(
        layer_kernel(senders, rows, capacity, col, hidden, share),
        out_shape=(
            buf((home_rows, col)),
            buf((2, home_rows), F32),
            buf((senders, LANES), F32),
            buf((width, hidden)),
            buf((width, hidden)),
            buf((hidden, width)),
        ),
        in_specs=[hbm] * 7,
        out_specs=[vmem] * 6,
        scratch_shapes=[
            buf(tokens.shape), buf(cotangent.shape), buf(routes.shape, routes.dtype), buf(router.shape),
            buf((width, hidden)), buf((width, hidden)), buf((hidden, width)),
            buf((slots, home_rows)), buf((rows, slots, col)), buf((slots, col)),
            buf((rows - 1, home_rows, col)), buf((rows - 1, slots // 2, col)),
            buf((senders, senders, LANES), F32), buf((senders, senders, LANES), F32),
            buf((slots, width)), buf((slots, width)),
            buf((slots, hidden)), buf((slots, hidden)), buf((slots, hidden)), buf((slots, width)),
            buf((senders, 8, LANES), F32), buf((senders, 8, LANES), F32), buf((seats, senders, 8, LANES), F32),
            buf((rows, slots, col)), buf((rows - 1, slots, col)), buf((slots, col)),
            buf((senders, width), F32), buf((senders, senders, LANES), F32),
            dma((7,)), dma((rows,)), dma((rows,)),
            dma((2 * rows, senders)), dma((2 * rows, senders)),
            dma((2, rows, senders)), dma((2, rows, senders)),
            dma((2, 2 * rows, senders)), dma((2, 2 * rows, senders)),
            dma((senders,)), dma((senders,)),
            dma((rows, senders)), dma((rows, senders)),
            dma((rows, senders)), dma((rows, senders)),
            dma((senders,)), dma((senders,)),
            dma((senders,)), dma((senders,)),
            dma((seats,)), dma((seats,)),
            dma((senders,)), dma((senders,)),
        ],
        compiler_params=pltpu.CompilerParams(has_side_effects=True, collective_id=0, vmem_limit_bytes=46 << 20),
        name="layer",
    )(tokens, cotangent, routes, router, w_gate, w_up, w_down)


def output_kernel(share):
    def body(tg, mix, rt, gg, ug, dg, tg_out, mix_out, rt_out, gg_out, ug_out, dg_out, sem):
        copies = [pltpu.make_async_copy(src, dst, sem.at[i])
                  for i, (src, dst) in enumerate(((gg, gg_out), (ug, ug_out), (dg, dg_out), (tg, tg_out), (mix, mix_out)))]
        for copy in copies:
            copy.start()
        offset = (lax.axis_index("ep") * lax.axis_size("tp") + lax.axis_index("tp")) * share % LANES
        total = jnp.zeros(rt_out.shape, F32)
        for start in range(0, LANES, share):
            total = total + jnp.where(offset == start, rt[:, start:start + share], 0.0)
        rt_out[...] = total
        for copy in copies:
            copy.wait()

    return body


def outputs(token_grad, mixing, router_rows, gate_grad, up_grad, down_grad, share):
    vmem = pl.BlockSpec(memory_space=pltpu.VMEM)
    hbm = pl.BlockSpec(memory_space=pl.ANY)
    like = [jax.ShapeDtypeStruct(x.shape, x.dtype) for x in (token_grad, mixing, router_rows, gate_grad, up_grad, down_grad)]
    like[2] = jax.ShapeDtypeStruct((router_rows.shape[0], share), F32)
    return pl.pallas_call(
        output_kernel(share),
        out_shape=like,
        in_specs=[vmem] * 6,
        out_specs=[hbm, hbm, vmem, hbm, hbm, hbm],
        scratch_shapes=[pltpu.SemaphoreType.DMA((5,))],
        compiler_params=pltpu.CompilerParams(vmem_limit_bytes=4 << 20),
        name="outputs",
    )(token_grad, mixing, router_rows, gate_grad, up_grad, down_grad)


def local(tokens, routes, router_matrix, cotangent, gate_proj, up_proj, down_proj):
    share = tokens.shape[1] // (lax.axis_size("ep") * lax.axis_size("tp"))
    results = layer(
        tokens, cotangent, routes.T, router_matrix.T, gate_proj[0], up_proj[0], down_proj[0]
    )
    token_grad, mixing, router_grad, gate_grad, up_grad, down_grad = outputs(*results, share)
    return (token_grad, mixing.T, router_grad.T, gate_grad[None], up_grad[None], down_grad[None])


def solution(mesh):
    return jax.shard_map(
        local,
        mesh=mesh,
        in_specs=(
            P("ep", None),
            P("ep", None),
            P(),
            P("ep", "tp"),
            P("ep", None, "tp"),
            P("ep", None, "tp"),
            P("ep", "tp", None),
        ),
        out_specs=(
            P("ep", "tp"),
            P("ep", None),
            P(("ep", "tp"), None),
            P("ep", None, "tp"),
            P("ep", None, "tp"),
            P("ep", "tp", None),
        ),
        check_vma=False,
    )
```

time: 150 us -> 105 us (0.70)
  Pallas kernels: 136 us -> 105 us
  local copies, waits for them, and re-layouts: 13.8 us -> 0 us
    pallas_call x1, Pallas kernels: 136 us -> 99.6 us  [layer(): pl.pallas_call(layer_kernel(senders, rows, capacity, col, hidden, share),...]
    unnamed x9 -> x0, local copies, waits for them, and re-layouts: 12.4 us -> none
    pallas_call x0 -> x1, Pallas kernels: none -> 4.89 us  [outputs(): pl.pallas_call(output_kernel(share), out_shape=like, in_specs=[vmem] * 6,...]
where the time goes in v2:
time: 105 us
  Pallas kernels  105 us (100%)
    pallas_call x1, Pallas kernels, layer(): pl.pallas_call(layer_kernel(senders, rows, capacity, col, hidden, share),...  99.6 us
    pallas_call x1, Pallas kernels, outputs(): pl.pallas_call(output_kernel(share), out_shape=like, in_specs=[vmem] * 6,...  4.89 us

profile of v2, /device:TPU:0, one launch (start us, length us, event | category | flops | bytes accessed | tf_op | source)
XLA Modules:
  0.0 105.3 jit_solution(672864052142393728)
XLA Ops:
  0.6 99.6 %layer.1 = (bf16[256,512]{1,0:T(8,128)(2,1)S(1)}, f32[2,256]{1,0:T(2,128)S(1)}, f32[8,128]{1,0:T(8,128)S(1)}, bf16[2048,896]{1,0:T(8,128)(2,1)S(1)}, bf16[2048,8...) custom-call(bf16[256,2048]{1,0:T(8,128)(2,1)} %tok_hbm.1, bf16[256,512]{1,0:T(8,128)(2,1)} %cot_hbm.1, ...), custom_call_target="tpu_custom_call" | custom-call | tf_op jit(solution)/shard_map/layer/pallas_call | solution.py:554
  100.3 4.9 %outputs.1 = (bf16[256,512]{1,0:T(8,128)(2,1)}, f32[2,256]{1,0:T(2,128)}, f32[8,64]{1,0:T(8,128)}, bf16[2048,896]{1,0:T(8,128)(2,1)}, bf16[2048,896]{1,0:T(8,128)(2,1)}, /*index=5*/bf16[896,2048]{1,0:T(8,128)(2,1)}) custom-call(bf16[256,512]{1,0:T(8,128)(2,1)S(1)} %get-tuple-element.18.tg, f32[2,256]{1,0:T(2,128)S(1)} %get-tuple-element.19.mix, ...), custom_call_target="tpu_custom_call" | custom-call | tf_op jit(solution)/shard_map/outputs/pallas_call | solution.py:616

commit v3 on v2

--- a/solution.py
+++ b/solution.py
@@ -10,8 +10,8 @@
 MESH = pl.DeviceIdType.MESH
 LANES = 128
 CHUNK = 256
-OUTER_TAKES = (2, 4, 4, 4, 4, 6, 7, 8, 8, 8, 8, 8, 8, 8, 8, 8, 8)
-INNER_TAKES = (2, 4, 4, 4, 4, 7, 8, 8, 8, 8, 8, 8, 8, 8, 8, 8, 8)
+OUTER_TAKES = (4, 6, 6, 6, 6, 7, 8, 8, 8, 8, 8, 8, 8)
+INNER_TAKES = (4, 6, 6, 6, 6, 6, 8, 8, 8, 8, 8, 8, 8)
 BF = jnp.bfloat16
 F32 = jnp.float32
 NN = (((1,), (0,)), ((), ()))
@@ -86,7 +86,7 @@
             return pair(me, k, senders)
 
         def raw_copy(step):
-            return remote(cot_ref, cot_raw.at[step - 1], raw_send.at[step], raw_recv.at[step], me, seat(step, core))
+            return remote(cot_ref, cot_raw.at[step - 1], raw_send.at[step - 1], raw_recv.at[step - 1], me, seat(step, core))
 
         barrier = pltpu.get_barrier_semaphore()
         each(1, senders, lambda k: pl.semaphore_signal(barrier, inc=1, device_id=(peer(k), tp), device_id_type=MESH))
@@ -101,9 +101,6 @@
             load.start()
         loads[0].wait()
         loads[3].wait()
-        pl.semaphore_wait(barrier, senders - 1 + seats - 1)
-        for step in range(1, rows):
-            raw_copy(step).start()
 
         ids = lax.broadcasted_iota(jnp.int32, (senders, tok_ref.shape[0]), 0)
         is_first = ids == routes_ref[0:1, :]
@@ -120,13 +117,12 @@
 
         loads[1].wait()
 
-        def choose_rows(i):
-            at = span(i, CHUNK)
-            cot_send[at, :] = dot(pick[at, :], cot_ref[...]).astype(BF)
-            for r in range(rows):
-                tok_send[r, at, :] = dot(pick[at, :], tok_ref[:, span(seat(r, core), col)]).astype(BF)
-
-        each(0, senders * capacity // CHUNK, choose_rows)
+        cot_send[...] = dot(pick[...], cot_ref[...]).astype(BF)
+        for r in range(rows):
+            tok_send[r] = dot(pick[...], tok_ref[:, span(seat(r, core), col)]).astype(BF)
+        pl.semaphore_wait(barrier, senders - 1 + seats - 1)
+        for step in range(1, rows):
+            raw_copy(step).start()
         own = span(me, capacity)
         tok_rows[own, :] = dot(pick[own, :], tok_ref[...]).astype(BF)
         cot_rows[own, span(tp, col)] = cot_send[own, :]
@@ -138,40 +134,39 @@
 
         mine = [(1, -j) for j in range(rows)]
         far = [(1, 0), (0, 0)]
-        early = far + [(0, j) for j in range(1, rows)]
-        near = early + [(1, -j) for j in range(1, rows)]
+        near = far + [(0, j) for j in range(1, rows)]
+        close = near + [(1, -j) for j in range(1, rows)]
         far_hops = [(a, j) for j in range(1, rows) for a in (1, 0)]
-        near_first = me // half * half
+        near_hops = [(1, j) for j in range(1, rows)]
+        close_first = my_chunk * per_chunk
 
         def ep_copy(i, dest, block):
-            array, which = near[i]
+            array, which = close[i]
             if array == 1 and which < 0:
-                source = cot_more.at[-which - 1, span(dest - near_first, capacity), :]
+                source = cot_more.at[-which - 1, span(dest - close_first, capacity), :]
             else:
                 source = (tok_send.at[which] if array == 0 else cot_send).at[span(dest, capacity), :]
             return remote(source, piece(arrays[array], block, seat(which, core)),
-                          ep_send.at[i, dest], ep_recv.at[i, block], dest, tp)
+                          ep_send.at[dest], ep_recv.at[min(i, 1), block], dest, tp)
+
+        def bulk(block, count, send, recv):
+            at = tok_rows.at[span(block, capacity), pl.ds(0, count * col)]
+            return remote(at, at, send, recv, me, partner)
 
         def mix_copy(dest, block):
-            return remote(mix_send.at[dest], mix_in.at[block], m_send.at[dest], m_recv.at[block], dest, tp)
+            return remote(mix_send.at[dest], mix_in.at[block], m_send.at[0], m_recv.at[block], dest, tp)
 
         def y_copy(array, step, block):
             at = piece(arrays[array], block, tp)
-            return remote(at, at, y_send.at[array, step, block], y_recv.at[array, step, block], me, seat(step, core))
+            return remote(at, at, y_send.at[block], y_recv.at[array, step - 1, block], me, seat(step, core))
 
         def y_arrival(array, step, block):
             at = piece(arrays[array], block, seat(-step, core))
-            return remote(at, at, y_send.at[array, step, block], y_recv.at[array, step, block], me, seat(step, core))
+            return remote(at, at, y_send.at[block], y_recv.at[array, step - 1, block], me, seat(step, core))
 
         def c_copy(array, step, block):
             at = piece(arrays[array], block, seat(step, core))
-            return remote(at, at, c_send.at[array, step + rows, block], c_recv.at[array, step + rows, block],
-                          me, partner)
-
-        def c_arrival(array, step, block):
-            at = piece(arrays[array], block, seat(step, 1 - core))
-            return remote(at, at, c_send.at[array, step + rows, block], c_recv.at[array, step + rows, block],
-                          me, partner)
+            return remote(at, at, c_send.at[block], c_recv.at[block], me, partner)
 
         inner = (my_chunk + my_chunk // 2) % 2
 
@@ -181,7 +176,12 @@
         def order(s):
             if chunks != 4:
                 return s
-            return jnp.where(inner == 1, choose(s, (3, 1, 0, 2)), choose(s, (0, 2, 1, 3)))
+            return jnp.where(inner == 1, choose(s, (0, 1, 2, 3)), choose(s, (0, 2, 1, 3)))
+
+        def take_order(s):
+            if chunks != 4:
+                return s
+            return jnp.where(inner == 1, s, choose(s, (2, 0, 1, 3)))
 
         def send(lo, hi):
             def action(k):
@@ -191,13 +191,12 @@
             return action
 
         def send_far(on):
-            flip = inner if chunks == 4 else 0
             for s in range(half // per_chunk, chunks):
-                start = pair(s, flip, chunks) * per_chunk
+                start = s * per_chunk
                 each(start, start + per_chunk * on, send(0, len(far)))
 
         c_copy(1, 0, me).start()
-        each(1, half, send(0, len(early)))
+        each(1, half, send(0, len(near)))
         loads[2].wait()
         logits = dot(router_ref[...], tok_ref[...], NT)
         chosen_first = jnp.sum(jnp.where(is_first, logits, 0.0), axis=0, keepdims=True)
@@ -212,20 +211,20 @@
         send_far(inner)
         for step in range(1, rows):
             raw_copy(step).wait_recv()
-            for n0 in range(0, half * capacity, CHUNK):
-                cot_more[step - 1, n0:n0 + CHUNK, :] = dot(
-                    pick[pl.ds(pl.multiple_of(near_first * capacity + n0, capacity), CHUNK), :], cot_raw[step - 1]
-                ).astype(BF)
-            cot_rows[own, span(seat(-step, core), col)] = cot_more[step - 1, span(me - near_first, capacity), :]
+            cot_more[step - 1] = dot(pick[span(my_chunk, chunk), :], cot_raw[step - 1]).astype(BF)
+            cot_rows[own, span(seat(-step, core), col)] = cot_more[step - 1, span(me - close_first, capacity), :]
             c_copy(1, -step, me).start()
-        each(1, half, send(len(early), len(near)))
+        each(1, per_chunk, send(len(near), len(close)))
         send_far(1 - inner)
 
         def take(items, hops):
             def action(j):
                 block = peer(j)
                 for i, (array, step) in enumerate(items):
-                    ep_copy(i, block, block).wait_recv()
+                    if i == 0:
+                        ep_copy(0, block, block).wait_recv()
+                    if i == 1:
+                        bulk(block, len(items) - 1, ep_send.at[block], ep_recv.at[1, block]).wait_recv()
                     for a, hop in hops:
                         if a == array and step == 0:
                             y_copy(array, hop, block).start()
@@ -245,8 +244,7 @@
         def settle(items, hops):
             def action(j):
                 block = peer(j)
-                for array, step in items + [(a, -s) for a, s in hops]:
-                    c_arrival(array, step, block).wait_recv()
+                bulk(block, len(items) + len(hops), c_send.at[block], c_recv.at[block]).wait_recv()
 
             return action
 
@@ -255,26 +253,18 @@
 
         def home_copy(dest, slot):
             return remote(piece(terms, dest, tp), home.at[span(slot, capacity), :],
-                          h_send.at[dest], h_recv.at[slot], dest, tp)
+                          h_send.at[0], h_recv.at[0], dest, tp)
 
         def part_copy(dest, slot):
-            return remote(mp_send.at[dest], mp_got.at[slot], p_send.at[dest], p_recv.at[slot], dest, tp)
+            return remote(mp_send.at[dest], mp_got.at[slot], p_send.at[0], p_recv.at[0], dest, tp)
 
         def rc_copy(step, block):
             return remote(piece(terms, block, seat(step, 1 - core)), c_buf.at[step, span(block, capacity), :],
-                          rc_send.at[step, block], rc_recv.at[step, block], me, partner)
+                          rc_send.at[block], rc_recv.at[step, block], me, partner)
 
         def ry_copy(step, block):
             return remote(piece(terms, block, seat(step, core)), y_buf.at[step - 1, span(block, capacity), :],
-                          ry_send.at[step, block], ry_recv.at[step, block], me, seat(step, core))
-
-        def start_back(j):
-            block = peer(j)
-            for step in range(1, rows):
-                rc_copy(step, block).start()
-
-        def rest_back(j):
-            rc_copy(0, peer(j)).start()
+                          ry_send.at[block], ry_recv.at[step - 1, block], me, seat(step, core))
 
         def first(j):
             block = peer(j)
@@ -333,63 +323,80 @@
                 line = to_row(total[i * capacity:(i + 1) * capacity, :])
                 mp_send[which * per_chunk + i, :, 0:capacity] = jnp.broadcast_to(line, (8, capacity))
 
-        def backward(which):
+        def backward(which, lo):
             at = span(which, chunk)
             gate_back = gb[at, :]
             up_back = ub[at, :]
-            for d0 in range(0, width, 512):
-                terms[at, d0:d0 + 512] = (
-                    dot(gate_back, wg[d0:d0 + 512, :], NT) + dot(up_back, wu[d0:d0 + 512, :], NT)
-                ).astype(BF)
-
-        def ranged(own_action, near_action, far_action):
+            for step in list(range(1, rows)) + [0]:
+                for side in (1 - core, core):
+                    cols = span(seat(step, side), col)
+                    terms[at, cols] = (dot(gate_back, wg[cols, :], NT) + dot(up_back, wu[cols, :], NT)).astype(BF)
+                for i in range(per_chunk):
+                    rc_copy(step, peer(lo + i)).start()
+
+        def ranged(own_action, close_action, near_action, far_action):
             def run(lo, hi):
                 if own_action is not None:
                     each(lo, jnp.minimum(hi, 1), own_action)
-                each(jnp.maximum(lo, 1), jnp.minimum(hi, half), near_action)
+                if close_action is not None:
+                    each(jnp.maximum(lo, 1), jnp.minimum(hi, per_chunk), close_action)
+                each(jnp.maximum(lo, per_chunk), jnp.minimum(hi, half), near_action)
                 each(jnp.maximum(lo, half), hi, far_action)
 
             return run
 
-        take_range = ranged(None, take(near, []), take(far, far_hops))
-        settle_range = ranged(settle(mine, []), settle(near, []), settle(far, far_hops))
+        take_range = ranged(None, take(close, []), take(near, near_hops), take(far, far_hops))
+        pass_range = ranged(None, None, pass_on(near_hops), pass_on(far_hops))
+        settle_range = ranged(settle(mine, []), settle(close, []), settle(near, near_hops), settle(far, far_hops))
         part = (per_chunk + 1) // 2
 
         def take_halves(lo, hi):
             def one(h):
-                start = order(h // 2) * per_chunk + h % 2 * part
+                start = take_order(h // 2) * per_chunk + h % 2 * part
                 take_range(start, start + part)
 
             each(lo, hi, one)
 
         def taken(s, point):
             def of(table):
-                return choose(s, [table[4 * i + point] for i in range(4)])
+                return choose(s, [table[3 * i + point] for i in range(4)])
 
             return jnp.where(inner == 1, of(INNER_TAKES), of(OUTER_TAKES))
 
         def take_point(s, point):
             take_halves(taken(s, point - 1), taken(s, point))
 
-        take_halves(0, 2)
-
-        def halves(first_step):
-            return [span(pair(my_chunk, order(s), chunks), chunk) for s in range(first_step, first_step + chunks // 2)]
-
-        def joined(ref, first_step, cols):
-            return jnp.concatenate([ref[at, cols] for at in halves(first_step)], axis=0)
+        take_halves(0, 4)
+
+        def joined(ref, steps, cols):
+            return jnp.concatenate([ref[span(pair(my_chunk, order(s), chunks), chunk), cols] for s in steps], axis=0)
+
+        first_half, second_half = range(chunks // 2), range(chunks // 2, chunks)
+
+        def down_early(i):
+            at = span(i, LANES)
+            x = joined(hs, range(chunks - 1), at)
+            for n0 in range(0, width, 512):
+                dg[at, n0:n0 + 512] = dot(x, joined(cot_rows, range(chunks - 1), slice(n0, n0 + 512)), TN).astype(BF)
+
+        def down(i):
+            at = span(i, LANES)
+            x = joined(hs, [chunks - 1], at)
+            for n0 in range(0, width, 512):
+                more = dot(x, joined(cot_rows, [chunks - 1], slice(n0, n0 + 512)), TN)
+                dg[at, n0:n0 + 512] = (dg[at, n0:n0 + 512].astype(F32) + more).astype(BF)
 
         def gate_up_early(i):
             at = span(i, CHUNK)
-            x = joined(tok_rows, 0, at)
-            gg[at, :] = dot(x, joined(gb, 0, slice(None)), TN).astype(BF)
-            ug[at, :] = dot(x, joined(ub, 0, slice(None)), TN).astype(BF)
+            x = joined(tok_rows, first_half, at)
+            gg[at, :] = dot(x, joined(gb, first_half, slice(None)), TN).astype(BF)
+            ug[at, :] = dot(x, joined(ub, first_half, slice(None)), TN).astype(BF)
 
         def gate_up(i):
             at = span(i, CHUNK)
-            x = joined(tok_rows, chunks // 2, at)
-            gg[at, :] = (gg[at, :].astype(F32) + dot(x, joined(gb, chunks // 2, slice(None)), TN)).astype(BF)
-            ug[at, :] = (ug[at, :].astype(F32) + dot(x, joined(ub, chunks // 2, slice(None)), TN)).astype(BF)
+            x = joined(tok_rows, second_half, at)
+            gg[at, :] = (gg[at, :].astype(F32) + dot(x, joined(gb, second_half, slice(None)), TN)).astype(BF)
+            ug[at, :] = (ug[at, :].astype(F32) + dot(x, joined(ub, second_half, slice(None)), TN)).astype(BF)
 
         def step_of(s):
             lo = order(s) * per_chunk
@@ -398,7 +405,8 @@
             earlier_chunk = order(jnp.maximum(s - 2, 0)) * per_chunk
             which = pair(my_chunk, order(s), chunks)
 
-            each(jnp.maximum(lo, half), hi, pass_on(far_hops))
+            each(0, jnp.where(s == chunks - 1, hidden // LANES, 0), down_early)
+            pass_range(lo, hi)
             settle_range(lo, hi)
             each(jnp.maximum(lo, 1), hi, arrive_mix)
 
@@ -410,44 +418,36 @@
             forward(which)
             each(jnp.maximum(lo, 1), hi, lambda j: part_copy(peer(j), me).start())
             take_point(s, 1)
-            each(earlier_chunk, earlier_chunk + jnp.where(s > 1, per_chunk, 0), second)
-            backward(which)
-            each(lo, hi, start_back)
-            each(lo, hi, rest_back)
+            each(earlier_chunk, earlier_chunk + jnp.where(s == 2, per_chunk, 0), second)
+            each(before, before + jnp.where(s > 1, per_chunk, 0), second)
+            backward(which, lo)
+            each(lo, hi, first)
             take_point(s, 2)
             each(0, jnp.where(s == chunks // 2 - 1, width // CHUNK, 0), gate_up_early)
             take_point(s, 3)
-            each(before, before + jnp.where(s == chunks - 1, per_chunk, 0), second)
-            each(lo, hi, first)
-            take_point(s, 4)
 
         each(0, chunks, step_of)
         mp_got[me] = mp_send[me]
-
-        def down(i):
-            at = span(i, LANES)
-            for n0 in range(0, width, 512):
-                dg[at, n0:n0 + 512] = dot(hs[:, at], cot_rows[:, n0:n0 + 512], TN).astype(BF)
 
         parts = width // CHUNK
         last = order(chunks - 1) * per_chunk
         middle = last + (per_chunk + 1) // 2
         each(0, parts // 2, gate_up)
+        others = pl.ds(0, senders - 1)
+
+        def all_parts():
+            return remote(mp_send.at[others], mp_got.at[others], p_send.at[0], p_recv.at[0], me, partner)
+
+        all_parts().wait_recv()
+        mix_all[0] = mp_got[...]
+
+        def t_copy(k):
+            return remote(mp_got, mix_all.at[k], t_send.at[k], t_recv.at[k], me, lax.rem(tp + k, seats))
+
+        for k in range(1, seats):
+            t_copy(k).start()
         each(last, middle, second)
         each(parts // 2, parts * 3 // 4, gate_up)
-        each(middle, last + per_chunk, second)
-        each(parts * 3 // 4, parts, gate_up)
-
-        each(1, senders, lambda j: part_copy(peer(j), peer(j)).wait_recv())
-        mix_all[0] = mp_got[...]
-
-        def t_copy(k):
-            return remote(mp_got, mix_all.at[k], t_send.at[k], t_recv.at[k], me, lax.rem(tp + k, seats))
-
-        for k in range(1, seats):
-            t_copy(k).start()
-        down_parts = hidden // LANES
-        each(0, (down_parts + 1) // 2, down)
         for k in range(1, seats):
             t_copy(k).wait()
 
@@ -472,64 +472,59 @@
             return span((dest * seats + tp) * share // LANES, LANES)
 
         def r_copy(dest, slot):
-            return remote(rt_full.at[:, rt_cols(dest)], rt_got.at[slot], r_send.at[dest], r_recv.at[slot], dest, tp)
+            return remote(rt_full.at[:, rt_cols(dest)], rt_got.at[slot], r_send.at[0], r_recv.at[0], dest, tp)
 
         each(1, senders, lambda k: r_copy(peer(k), me).start())
         rt_got[me] = rt_full[:, rt_cols(me)]
-        each((down_parts + 1) // 2, down_parts, down)
-
-        def close(items, hops):
+        each(middle, last + per_chunk, second)
+        each(parts * 3 // 4, parts, gate_up)
+        each(0, hidden // LANES, down)
+
+        def finish(items, hops):
             def action(j):
                 block = peer(j)
-                for array, step in items + [(a, -s) for a, s in hops]:
-                    c_copy(array, step, block).wait_send()
-                for array, step in hops:
-                    y_copy(array, step, block).wait_send()
+                bulk(block, len(items) + len(hops), c_send.at[block], c_recv.at[block]).wait_send()
+                if hops:
+                    bulk(block, len(hops), y_send.at[block], y_recv.at[0, 0, block]).wait_send()
+                if items is not mine:
+                    bulk(block, len(items), ep_send.at[block], ep_recv.at[0, block]).wait_send()
 
             return action
 
         for step in range(1, rows):
             raw_copy(step).wait_send()
-        close(mine, [])(0)
-        each(1, half, close(near, []))
-        each(half, senders, close(far, far_hops))
+        finish(mine, [])(0)
+        each(1, per_chunk, finish(close, []))
+        each(per_chunk, half, finish(near, near_hops))
+        each(half, senders, finish(far, far_hops))
 
         def close_back(j):
             block = peer(j)
-            for step in range(rows):
-                rc_copy(step, block).wait_send()
-            for step in range(1, rows):
-                ry_copy(step, block).wait_send()
+            bulk(block, rows, rc_send.at[block], rc_recv.at[0, block]).wait_send()
+            bulk(block, rows - 1, ry_send.at[block], ry_recv.at[0, block]).wait_send()
 
         each(0, senders, close_back)
-
-        def close_dispatch(count):
-            def action(k):
-                dest = peer(k)
-                for i in range(count):
-                    ep_copy(i, dest, me).wait_send()
-                mix_copy(dest, me).wait_send()
-
-            return action
-
-        each(1, half, close_dispatch(len(near)))
-        each(half, senders, close_dispatch(len(far)))
+        remote(mix_send.at[others], mix_in.at[others], m_send.at[0], m_recv.at[0], me, partner).wait_send()
+        all_parts().wait_send()
+
+        def all_home():
+            at = home.at[pl.ds(0, (senders - 1) * capacity), :]
+            return remote(at, at, h_send.at[0], h_recv.at[0], me, partner)
+
+        def all_router():
+            at = rt_got.at[others]
+            return remote(at, at, r_send.at[0], r_recv.at[0], me, partner)
 
         home[own, :] = terms[own, span(tp, col)]
-        each(1, senders, lambda k: home_copy(peer(k), peer(k)).wait_recv())
+        all_home().wait_recv()
         cols = router_ref[:, span(tp, col)]
         tg_out[...] = (
             dot(pick[...], home[...], TN) + dot(route_grad, jnp.concatenate([cols, cols, cols], axis=0), TN)
         ).astype(BF)
-        each(1, senders, lambda k: r_copy(peer(k), peer(k)).wait_recv())
+        all_router().wait_recv()
         rt_out[...] = jnp.sum(rt_got[...], axis=0)
-
-        def close_sends(dest):
-            part_copy(dest, me).wait_send()
-            home_copy(dest, me).wait_send()
-            r_copy(dest, me).wait_send()
-
-        each(1, senders, lambda k: close_sends(peer(k)))
+        all_home().wait_send()
+        all_router().wait_send()
 
     return body
 
@@ -567,24 +562,24 @@
             buf(tokens.shape), buf(cotangent.shape), buf(routes.shape, routes.dtype), buf(router.shape),
             buf((width, hidden)), buf((width, hidden)), buf((hidden, width)),
             buf((slots, home_rows)), buf((rows, slots, col)), buf((slots, col)),
-            buf((rows - 1, home_rows, col)), buf((rows - 1, slots // 2, col)),
+            buf((rows - 1, home_rows, col)), buf((rows - 1, max(CHUNK, capacity), col)),
             buf((senders, senders, LANES), F32), buf((senders, senders, LANES), F32),
             buf((slots, width)), buf((slots, width)),
             buf((slots, hidden)), buf((slots, hidden)), buf((slots, hidden)), buf((slots, width)),
             buf((senders, 8, LANES), F32), buf((senders, 8, LANES), F32), buf((seats, senders, 8, LANES), F32),
             buf((rows, slots, col)), buf((rows - 1, slots, col)), buf((slots, col)),
             buf((senders, width), F32), buf((senders, senders, LANES), F32),
-            dma((7,)), dma((rows,)), dma((rows,)),
-            dma((2 * rows, senders)), dma((2 * rows, senders)),
-            dma((2, rows, senders)), dma((2, rows, senders)),
-            dma((2, 2 * rows, senders)), dma((2, 2 * rows, senders)),
+            dma((7,)), dma((rows - 1,)), dma((rows - 1,)),
+            dma((senders,)), dma((2, senders)),
+            dma((senders,)), dma((2, rows - 1, senders)),
             dma((senders,)), dma((senders,)),
-            dma((rows, senders)), dma((rows, senders)),
-            dma((rows, senders)), dma((rows, senders)),
-            dma((senders,)), dma((senders,)),
-            dma((senders,)), dma((senders,)),
+            dma((1,)), dma((senders,)),
+            dma((senders,)), dma((rows, senders)),
+            dma((senders,)), dma((rows - 1, senders)),
+            dma((1,)), dma((1,)),
+            dma((1,)), dma((1,)),
             dma((seats,)), dma((seats,)),
-            dma((senders,)), dma((senders,)),
+            dma((1,)), dma((1,)),
         ],
         compiler_params=pltpu.CompilerParams(has_side_effects=True, collective_id=0, vmem_limit_bytes=46 << 20),
         name="layer",

time: 105 us -> 101 us (0.962); the launches traced: 105 us -> 99.8 us
  Pallas kernels: 105 us -> 99.1 us
    pallas_call x1, Pallas kernels: 99.6 us -> 94.3 us  [layer(): pl.pallas_call(layer_kernel(senders, rows, capacity, col, hidden, share),...]
where the time goes in v3:
time: 101 us; the launch traced here: 99.8 us
  Pallas kernels  99.1 us (98%)
    pallas_call x1, Pallas kernels, layer(): pl.pallas_call(layer_kernel(senders, rows, capacity, col, hidden, share),...  94.3 us
    pallas_call x1, Pallas kernels, outputs(): pl.pallas_call(output_kernel(share), out_shape=like, in_specs=[vmem] * 6,...  4.89 us

profile of v3, /device:TPU:0, one launch (start us, length us, event | category | flops | bytes accessed | tf_op | source)
XLA Modules:
  0.0 99.8 jit_solution(7632467900930367717)
XLA Ops:
  0.6 94.3 %layer.1 = (bf16[256,512]{1,0:T(8,128)(2,1)S(1)}, f32[2,256]{1,0:T(2,128)S(1)}, f32[8,128]{1,0:T(8,128)S(1)}, bf16[2048,896]{1,0:T(8,128)(2,1)S(1)}, bf16[2048,8...) custom-call(bf16[256,2048]{1,0:T(8,128)(2,1)} %tok_hbm.1, bf16[256,512]{1,0:T(8,128)(2,1)} %cot_hbm.1, ...), custom_call_target="tpu_custom_call" | custom-call | tf_op jit(solution)/shard_map/layer/pallas_call | solution.py:549
  94.9 4.9 %outputs.1 = (bf16[256,512]{1,0:T(8,128)(2,1)}, f32[2,256]{1,0:T(2,128)}, f32[8,64]{1,0:T(8,128)}, bf16[2048,896]{1,0:T(8,128)(2,1)}, bf16[2048,896]{1,0:T(8,128)(2,1)}, /*index=5*/bf16[896,2048]{1,0:T(8,128)(2,1)}) custom-call(bf16[256,512]{1,0:T(8,128)(2,1)S(1)} %get-tuple-element.18.tg, f32[2,256]{1,0:T(2,128)S(1)} %get-tuple-element.19.mix, ...), custom_call_target="tpu_custom_call" | custom-call | tf_op jit(solution)/shard_map/outputs/pallas_call | solution.py:611

commit v4 on v3

--- a/solution.py
+++ b/solution.py
@@ -10,7 +10,7 @@
 MESH = pl.DeviceIdType.MESH
 LANES = 128
 CHUNK = 256
-OUTER_TAKES = (4, 6, 6, 6, 6, 7, 8, 8, 8, 8, 8, 8, 8)
+OUTER_TAKES = (4, 4, 6, 6, 6, 7, 8, 8, 8, 8, 8, 8, 8)
 INNER_TAKES = (4, 6, 6, 6, 6, 6, 8, 8, 8, 8, 8, 8, 8)
 BF = jnp.bfloat16
 F32 = jnp.float32
@@ -398,6 +398,9 @@
             gg[at, :] = (gg[at, :].astype(F32) + dot(x, joined(gb, second_half, slice(None)), TN)).astype(BF)
             ug[at, :] = (ug[at, :].astype(F32) + dot(x, joined(ub, second_half, slice(None)), TN)).astype(BF)
 
+        cuts = [hidden // LANES * 3 // 7, hidden // LANES * 5 // 7, hidden // LANES]
+        ready = width // CHUNK * 5 // 8
+
         def step_of(s):
             lo = order(s) * per_chunk
             hi = lo + per_chunk
@@ -405,8 +408,9 @@
             earlier_chunk = order(jnp.maximum(s - 2, 0)) * per_chunk
             which = pair(my_chunk, order(s), chunks)
 
-            each(0, jnp.where(s == chunks - 1, hidden // LANES, 0), down_early)
-            pass_range(lo, hi)
+            each(0, jnp.where(s == chunks - 1, cuts[0], 0), down_early)
+            pass_range(jnp.where(s == 2, hi, lo), hi)
+            each(cuts[0], jnp.where(s == chunks - 1, cuts[1], cuts[0]), down_early)
             settle_range(lo, hi)
             each(jnp.maximum(lo, 1), hi, arrive_mix)
 
@@ -423,8 +427,11 @@
             backward(which, lo)
             each(lo, hi, first)
             take_point(s, 2)
-            each(0, jnp.where(s == chunks // 2 - 1, width // CHUNK, 0), gate_up_early)
+            each(0, jnp.where(s == chunks // 2 - 1, ready, 0), gate_up_early)
             take_point(s, 3)
+            coming = order(min(2, chunks - 1)) * per_chunk + per_chunk
+            pass_range(jnp.where(s == 1, coming - per_chunk, coming), coming)
+            each(ready, jnp.where(s == chunks // 2 - 1, width // CHUNK, ready), gate_up_early)
 
         each(0, chunks, step_of)
         mp_got[me] = mp_send[me]
@@ -478,6 +485,7 @@
         rt_got[me] = rt_full[:, rt_cols(me)]
         each(middle, last + per_chunk, second)
         each(parts * 3 // 4, parts, gate_up)
+        each(cuts[1], cuts[2], down_early)
         each(0, hidden // LANES, down)
 
         def finish(items, hops):

time: 101 us -> 99.9 us (0.989)
  no operation moved by 1% of the time
where the time goes in v4:
time: 99.9 us; the launch traced here: 99.2 us
  Pallas kernels  98.6 us (99%)
    pallas_call x1, Pallas kernels, layer(): pl.pallas_call(layer_kernel(senders, rows, capacity, col, hidden, share),...  93.7 us
    pallas_call x1, Pallas kernels, outputs(): pl.pallas_call(output_kernel(share), out_shape=like, in_specs=[vmem] * 6,...  4.89 us

profile of v4, /device:TPU:0, one launch (start us, length us, event | category | flops | bytes accessed | tf_op | source)
XLA Modules:
  0.0 99.2 jit_solution(6601340431931494537)
XLA Ops:
  0.6 93.7 %layer.1 = (bf16[256,512]{1,0:T(8,128)(2,1)S(1)}, f32[2,256]{1,0:T(2,128)S(1)}, f32[8,128]{1,0:T(8,128)S(1)}, bf16[2048,896]{1,0:T(8,128)(2,1)S(1)}, bf16[2048,8...) custom-call(bf16[256,2048]{1,0:T(8,128)(2,1)} %tok_hbm.1, bf16[256,512]{1,0:T(8,128)(2,1)} %cot_hbm.1, ...), custom_call_target="tpu_custom_call" | custom-call | tf_op jit(solution)/shard_map/layer/pallas_call | solution.py:557
  94.3 4.9 %outputs.1 = (bf16[256,512]{1,0:T(8,128)(2,1)}, f32[2,256]{1,0:T(2,128)}, f32[8,64]{1,0:T(8,128)}, bf16[2048,896]{1,0:T(8,128)(2,1)}, bf16[2048,896]{1,0:T(8,128)(2,1)}, /*index=5*/bf16[896,2048]{1,0:T(8,128)(2,1)}) custom-call(bf16[256,512]{1,0:T(8,128)(2,1)S(1)} %get-tuple-element.18.tg, f32[2,256]{1,0:T(2,128)S(1)} %get-tuple-element.19.mix, ...), custom_call_target="tpu_custom_call" | custom-call | tf_op jit(solution)/shard_map/outputs/pallas_call | solution.py:619
